TPU v7x, 32 devices: a whole 2x2x4 slice. The times are simulated.
32 devices in a mesh: sp: 16 (over z, y, x), tp: 2 (over core).
Axes of the slice: x: 2, y: 2, z: 4, core: 2. Of those that a mesh axis runs over, the one named last changes fastest.
Arguments:
- tokens: bfloat16 [3584, 2048], P('sp', 'tp'), may hold values from -6 to 6
- norm_gain: float32 [2048], replicated, may hold values from 0.1 to 1.9
- query_weight: bfloat16 [2048, 2048], P('sp', 'tp'), may hold values from -0.125 to 0.125
- key_weight: bfloat16 [2048, 1024], P('sp', 'tp'), may hold values from -0.125 to 0.125
- value_weight: bfloat16 [2048, 1024], P('sp', 'tp'), may hold values from -0.125 to 0.125
- glu_value_weight: bfloat16 [2048, 1536], P('sp', 'tp'), may hold values from -0.125 to 0.125
- glu_gate_weight: bfloat16 [2048, 1536], P('sp', 'tp'), may hold values from -0.125 to 0.125
- query_gain: float32 [64], replicated, may hold values from 1.2 to 1.6
- key_gain: float32 [64], replicated, may hold values from 1.1 to 1.4
- lambdas: float32 [16], P('tp'), may hold values from 0.3 to 0.8
- head_gain: float32 [128], replicated, may hold values from 0.1 to 1.9
- conv_weight: float32 [31, 1536], P(None, 'tp'), may hold values from -11 to 11
- channel_gain: float32 [1536], P('tp'), may hold values from 0.1 to 1.9
- attn_out_weight: bfloat16 [2048, 2048], P('sp', 'tp'), may hold values from -0.09375 to 0.09375
- conv_out_weight: bfloat16 [2048, 1536], P('sp', 'tp'), may hold values from -0.09375 to 0.09375
Outputs:
- mixed: bfloat16 [3584, 2048], P(('sp', 'tp'))
All inputs are finite; a program needn't handle non-finite values.
Results may differ from a plain program's by a relative error of at most 0.014.
Values may be sent and summed in bfloat16 or wider, within the bound.
A program may use at most 128 MiB of HBM per device.

v0:
```python
import jax
import jax.numpy as jnp
from jax import lax
from jax.sharding import PartitionSpec as P

HEAD_DIM = 64
C_CH = 1536
CONV_W = 31


EPS = 1e-06
LAMBDA_INIT = 0.2


def with_halo(cells, sides, width):
    for axis, dim in sides:
        count = lax.axis_size(axis)
        ends = count - 1
        head = lax.slice_in_dim(cells, 0, width, axis=dim)
        tail = lax.slice_in_dim(cells, cells.shape[dim] - width, cells.shape[dim], axis=dim)
        cells = jnp.concatenate(
            [
                lax.ppermute(tail, axis, [(i, (i + 1) % count) for i in range(ends)]),
                cells,
                lax.ppermute(head, axis, [((i + 1) % count, i) for i in range(ends)]),
            ],
            axis=dim,
        )
    return cells


def rms_scale(values, gain):
    return values * lax.rsqrt(jnp.mean(values * values, axis=-1, keepdims=True) + EPS) * gain


def contract_last(left, right):
    return lax.dot_general(
        left, right, (((1,), (1,)), ((), ())), preferred_element_type=jnp.float32
    )


def local(
    tokens,
    norm_gain,
    query_weight,
    key_weight,
    value_weight,
    glu_value_weight,
    glu_gate_weight,
    query_gain,
    key_gain,
    lambdas,
    head_gain,
    conv_weight,
    channel_gain,
    attn_out_weight,
    conv_out_weight,
):
    gathered = lax.all_gather(tokens, "tp", axis=1, tiled=True).astype(jnp.float32)
    normed = rms_scale(gathered, norm_gain).astype(jnp.bfloat16)
    tok_rows, model_width = normed.shape
    pieces = (
        lax.all_gather(query_weight, "sp", axis=0, tiled=True),
        lax.all_gather(key_weight, "sp", axis=0, tiled=True),
        lax.all_gather(value_weight, "sp", axis=0, tiled=True),
        lax.all_gather(glu_value_weight, "sp", axis=0, tiled=True),
        lax.all_gather(glu_gate_weight, "sp", axis=0, tiled=True),
    )
    projected = tuple(
        (jnp.dot(normed, w_piece, preferred_element_type=jnp.float32) for w_piece in pieces)
    )
    q_heads = query_weight.shape[1] // (2 * HEAD_DIM)
    kv_heads = key_weight.shape[1] // (2 * HEAD_DIM)
    group = q_heads // kv_heads
    queries = projected[0].reshape(tok_rows, q_heads, 2, HEAD_DIM)
    query_normed = rms_scale(queries, query_gain).astype(jnp.bfloat16)
    query_blocks = query_normed.reshape(tok_rows, kv_heads, group, 2, HEAD_DIM).transpose(
        1, 2, 3, 0, 4
    )
    keys = projected[1].reshape(tok_rows, kv_heads, 2, HEAD_DIM)
    key_rows = (
        rms_scale(keys, key_gain).astype(jnp.bfloat16).reshape(tok_rows, kv_heads * 2 * HEAD_DIM)
    )
    value_rows = projected[2].astype(jnp.bfloat16)

    def attend_block(carry, key_block, value_block):
        run_max, run_sum, numer = carry
        key_count = key_block.shape[0]
        key_heads = key_block.reshape(key_count, kv_heads, 2, HEAD_DIM).transpose(1, 2, 0, 3)
        value_heads = value_block.reshape(key_count, kv_heads, 2 * HEAD_DIM).transpose(1, 0, 2)
        scores = jnp.einsum(
            "kgprd,kpnd->kgprn", query_blocks, key_heads, preferred_element_type=jnp.float32
        ) * HEAD_DIM ** (-0.5)
        new_max = jnp.maximum(run_max, jnp.max(scores, axis=-1))
        expo = jnp.exp(scores - new_max[..., None])
        factor = jnp.exp(run_max - new_max)
        run_sum = run_sum * factor + jnp.sum(expo, axis=-1)
        numer = numer * factor[..., None] + jnp.einsum(
            "kgprn,knd->kgprd",
            expo.astype(jnp.bfloat16),
            value_heads,
            preferred_element_type=jnp.float32,
        )
        return (new_max, run_sum, numer)

    start_carry = (
        jnp.full((kv_heads, group, 2, tok_rows), -jnp.inf, jnp.float32),
        jnp.zeros((kv_heads, group, 2, tok_rows), jnp.float32),
        jnp.zeros((kv_heads, group, 2, tok_rows, 2 * HEAD_DIM), jnp.float32),
    )
    carry = start_carry
    pieces = (
        lax.all_gather(key_rows, "sp", axis=0, tiled=True),
        lax.all_gather(value_rows, "sp", axis=0, tiled=True),
    )
    key_count = pieces[0].shape[0]
    step_rows = key_count
    while step_rows > 1024 and step_rows % 2 == 0:
        step_rows = step_rows // 2
    turn_count = key_count // step_rows
    key_steps = pieces[0].reshape(turn_count, step_rows, pieces[0].shape[1])
    value_steps = pieces[1].reshape(turn_count, step_rows, pieces[1].shape[1])

    def one_turn(inner, both):
        return (attend_block(inner, both[0], both[1]), None)

    carry, unused = lax.scan(one_turn, carry, (key_steps, value_steps))
    run_max, run_sum, numer = carry
    ratio = numer / run_sum[..., None]
    weight_two = lambdas.reshape(kv_heads, group, 1, 1)
    difference = ratio[:, :, 0] - weight_two * ratio[:, :, 1]
    att_rows = difference.transpose(2, 0, 1, 3).reshape(tok_rows, q_heads, 2 * HEAD_DIM)
    att_normed = (rms_scale(att_rows, head_gain) * (1.0 - LAMBDA_INIT)).astype(jnp.bfloat16)
    att_out = att_normed.reshape(tok_rows, q_heads * 2 * HEAD_DIM)
    glu_rows = (projected[3] * jax.nn.sigmoid(projected[4])).astype(jnp.bfloat16)
    padded = with_halo(glu_rows, (("sp", 0),), CONV_W // 2)
    conv_sum = jnp.zeros((tok_rows, glu_rows.shape[1]), jnp.float32)
    for offset in range(CONV_W):
        conv_sum = conv_sum + conv_weight[offset] * padded[offset : offset + tok_rows].astype(
            jnp.float32
        )
    squares = lax.psum(jnp.sum(conv_sum * conv_sum, axis=1), "tp")
    scaled = conv_sum * lax.rsqrt(squares / C_CH + EPS)[:, None] * channel_gain
    conv_out = jax.nn.silu(scaled).astype(jnp.bfloat16)
    pieces = (
        lax.all_gather(attn_out_weight, "sp", axis=0, tiled=True),
        lax.all_gather(conv_out_weight, "sp", axis=0, tiled=True),
    )
    partial_term = contract_last(att_out, pieces[0]) + contract_last(conv_out, pieces[1])
    return lax.psum_scatter(
        partial_term.astype(jnp.bfloat16), "tp", scatter_dimension=0, tiled=True
    )


def solution(mesh):
    return jax.shard_map(
        local,
        mesh=mesh,
        in_specs=(
            P("sp", "tp"),
            P(),
            P("sp", "tp"),
            P("sp", "tp"),
            P("sp", "tp"),
            P("sp", "tp"),
            P("sp", "tp"),
            P(),
            P(),
            P("tp"),
            P(),
            P(None, "tp"),
            P("tp"),
            P("sp", "tp"),
            P("sp", "tp"),
        ),
        out_specs=P(("sp", "tp"), None),
        check_vma=False,
    )
```

profile of v0, /device:TPU:0, one launch (start us, length us, event | category | flops | bytes accessed | tf_op | source)
XLA Modules:
  0.0 660.4 jit_solution(10927576738663666540)
XLA Ops:
  6.5 0.7 all-gather.10.cloned.1.call-update
  7.3 0.7 all-gather.16.cloned.1.call-update
  8.1 0.7 all-gather.24.cloned.1.call-update
  10.7 2.8 all_gather.30
  13.7 59.5 %all-gather.10.cloned.1.call-done = bf16[2048,512]{1,0:T(8,128)(2,1)} async-done(((bf16[128,512]{1,0:T(8,128)(2,1)}), bf16[2048,512]{1,0:T(8,128)(2,1)}) %all-gather.10.cloned.1.call-update) | async-done | bytes 2097168 | tf_op jit(solution)/shard_map/all_gather | solution.py:64
  73.2 2.3 fusion.72
  76.1 0.8 multiply_convert_fusion.2
  76.9 58.3 %all-gather.16.cloned.1.call-done = bf16[2048,512]{1,0:T(8,128)(2,1)} async-done(((bf16[128,512]{1,0:T(8,128)(2,1)}), bf16[2048,512]{1,0:T(8,128)(2,1)}) %all-gather.16.cloned.1.call-update) | async-done | bytes 2097168 | tf_op jit(solution)/shard_map/all_gather | solution.py:65
  135.2 3.0 convolution_convert_fusion
  138.3 0.7 all-gather.20.cloned.1.call-update
  139.0 0.7 all-gather.26.cloned.1.call-update
  140.0 64.7 %all-gather.24.cloned.1.call-done = bf16[2048,768]{1,0:T(8,128)(2,1)} async-done(((bf16[128,768]{1,0:T(8,128)(2,1)}), bf16[2048,768]{1,0:T(8,128)(2,1)}) %all-gather.24.cloned.1.call-update) | async-done | bytes 3145744 | tf_op jit(solution)/shard_map/all_gather | solution.py:67
  204.7 2.9 fusion.17
  207.6 66.2 %all-gather.22.cloned.1.call-done = bf16[2048,768]{1,0:T(8,128)(2,1)} async-done(((bf16[128,768]{1,0:T(8,128)(2,1)}), bf16[2048,768]{1,0:T(8,128)(2,1)}) %all-gather.22.cloned.1.call-update) | async-done | bytes 3145744 | tf_op jit(solution)/shard_map/all_gather | solution.py:66
  273.8 2.8 fusion.18
  276.6 3.4 collective-permute-start
  280.0 1.3 collective-permute-start.1
  281.5 4.2 collective-permute-done.1
  285.7 4.5 multiply_reduce_fusion.1
  290.2 2.6 psum.7
  292.8 57.6 %all-gather.14.cloned.1.call-done = bf16[2048,1024]{1,0:T(8,128)(2,1)} async-done(((bf16[128,1024]{1,0:T(8,128)(2,1)}), bf16[2048,1024]{1,0:T(8,128)(2,1)}) %all-gather.14.cloned.1.call-update) | async-done | bytes 4194320 | tf_op jit(solution)/shard_map/all_gather | solution.py:63
  350.4 3.4 fusion.73
  355.2 68.1 %all-gather.12.cloned.1.call-done = bf16[3584,512]{1,0:T(8,128)(2,1)} async-done(((bf16[224,512]{1,0:T(8,128)(2,1)}), bf16[3584,512]{1,0:T(8,128)(2,1)}) %all-gather.12.cloned.1.call-update) | async-done | bytes 3670032 | tf_op jit(solution)/shard_map/all_gather | solution.py:113
  423.3 72.9 %all-gather.18.cloned.1.call-done = bf16[3584,512]{1,0:T(8,128)(2,1)} async-done(((bf16[224,512]{1,0:T(8,128)(2,1)}), bf16[3584,512]{1,0:T(8,128)(2,1)}) %all-gather.18.cloned.1.call-update) | async-done | bytes 3670032 | tf_op jit(solution)/shard_map/all_gather | solution.py:114
  496.2 99.3 %while.15 = (s32[]{:T(128)}, f32[4,2,2,224]{3,1,2,0:T(2,128)S(1)}, f32[4,2,2,224]{3,1,2,0:T(2,128)S(1)}, f32[4,2,2,224,128]{4,3,2,1,0:T(8,128)}, bf16[4,896,512]...) while((s32[]{:T(128)}, f32[4,2,2,224]{3,1,2,0:T(2,128)S(1)}, ...), condition=%wide.region_6.7_spmd.clone, body=%wide.region_3.6_spmd.clone.sunk | while | flops 1253787136 | bytes 53917800 | solution.py:127
  496.2 1.6 constant_dynamic-slice_fusion.3
  498.4 6.5 bitcast_reduce_fusion.4
  504.9 8.6 %fusion.96 = (bf16[4,2,2,224,896]{4,3,1,2,0:T(8,128)(2,1)}, f32[4,2,2,224]{3,1,2,0:T(2,128)S(1)}) fusion(f32[4,2,896,2,224]{2,4,3,1,0:T(8,128)} %get-tuple-element.199, f32[4,2,2,224]{3,1,2,0:T(2,128)S(1)} %fusion.95), kind=kLoop, calls=%fused_computation.3.clone.1 | loop fusion | flops 12841472 | bytes 19296256 | tf_op jit(solution)/shard_map/while/body/eval_jaxpr/convert_element_type | solution.py:100
  514.8 5.9 fusion.98
  520.8 1.6 constant_dynamic-slice_fusion.3
  522.9 6.5 bitcast_reduce_fusion.4
  529.5 8.5 %fusion.96 = (bf16[4,2,2,224,896]{4,3,1,2,0:T(8,128)(2,1)}, f32[4,2,2,224]{3,1,2,0:T(2,128)S(1)}) fusion(f32[4,2,896,2,224]{2,4,3,1,0:T(8,128)} %get-tuple-element.199, f32[4,2,2,224]{3,1,2,0:T(2,128)S(1)} %fusion.95), kind=kLoop, calls=%fused_computation.3.clone.1 | loop fusion | flops 12841472 | bytes 19296256 | tf_op jit(solution)/shard_map/while/body/eval_jaxpr/convert_element_type | solution.py:100
  539.2 6.4 fusion.98
  545.7 1.6 constant_dynamic-slice_fusion.3
  547.9 6.5 bitcast_reduce_fusion.4
  554.4 8.5 %fusion.96 = (bf16[4,2,2,224,896]{4,3,1,2,0:T(8,128)(2,1)}, f32[4,2,2,224]{3,1,2,0:T(2,128)S(1)}) fusion(f32[4,2,896,2,224]{2,4,3,1,0:T(8,128)} %get-tuple-element.199, f32[4,2,2,224]{3,1,2,0:T(2,128)S(1)} %fusion.95), kind=kLoop, calls=%fused_computation.3.clone.1 | loop fusion | flops 12841472 | bytes 19296256 | tf_op jit(solution)/shard_map/while/body/eval_jaxpr/convert_element_type | solution.py:100
  564.2 6.5 fusion.98
  570.6 1.6 constant_dynamic-slice_fusion.3
  572.8 6.5 bitcast_reduce_fusion.4
  579.3 8.5 %fusion.96 = (bf16[4,2,2,224,896]{4,3,1,2,0:T(8,128)(2,1)}, f32[4,2,2,224]{3,1,2,0:T(2,128)S(1)}) fusion(f32[4,2,896,2,224]{2,4,3,1,0:T(8,128)} %get-tuple-element.199, f32[4,2,2,224]{3,1,2,0:T(2,128)S(1)} %fusion.95), kind=kLoop, calls=%fused_computation.3.clone.1 | loop fusion | flops 12841472 | bytes 19296256 | tf_op jit(solution)/shard_map/while/body/eval_jaxpr/convert_element_type | solution.py:100
  589.1 6.5 fusion.98
  595.6 2.0 broadcast_divide_fusion
  598.1 0.7 copy.34
  598.8 0.7 reshape.95
  600.0 3.7 fusion.26
  603.8 38.7 %all-gather.26.cloned.1.call-done = bf16[2048,768]{1,0:T(8,128)(2,1)} async-done(((bf16[128,768]{1,0:T(8,128)(2,1)}), bf16[2048,768]{1,0:T(8,128)(2,1)}) %all-gather.26.cloned.1.call-update) | async-done | bytes 3145744 | tf_op jit(solution)/shard_map/all_gather | solution.py:147
  642.5 4.1 fusion.11
  646.6 6.9 %reduce-scatter.2.cloned.1.call-done = bf16[112,2048]{1,0:T(8,128)(2,1)} async-done(((bf16[224,2048]{1,0:T(8,128)(2,1)}), bf16[112,2048]{1,0:T(8,128)(2,1)}) %reduce-scatter.2.cloned.1.call-update) | async-done | bytes 458768 | tf_op jit(solution)/shard_map/reduce_scatter | solution.py:150
  (91 shorter events, 13.1 us)
Async XLA Ops:
  6.5 133.2 %copy-start = (f32[128]{0:T(128)S(1)}, f32[128]{0:T(128)}, u32[]{:S(2)}) copy-start(f32[128]{0:T(128)} %param.27) | copy-start | bytes 1540
  6.5 66.7 %copy-start.6 = (f32[2048]{0:T(1024)S(1)}, f32[2048]{0:T(1024)}, u32[]{:S(2)}) copy-start(f32[2048]{0:T(1024)} %param.18) | copy-start | bytes 24580
  6.5 66.7 %all-gather.10.cloned.1.call-start = ((), (), s32[]{:S(2)}) async-start(), calls=%async_computation.1 | async-start | bytes 2228224 | tf_op jit(solution)/shard_map/all_gather | solution.py:64
  7.3 128.0 %all-gather.16.cloned.1.call-start = ((), (), s32[]{:S(2)}) async-start(), calls=%async_computation.4 | async-start | bytes 2228224 | tf_op jit(solution)/shard_map/all_gather | solution.py:65
  8.0 196.7 %all-gather.24.cloned.1.call-start = ((), (), s32[]{:S(2)}) async-start(), calls=%async_computation.8 | async-start | bytes 3342336 | tf_op jit(solution)/shard_map/all_gather | solution.py:67
  8.7 265.0 %all-gather.22.cloned.1.call-start = ((), (), s32[]{:S(2)}) async-start(), calls=%async_computation.7 | async-start | bytes 3342336 | tf_op jit(solution)/shard_map/all_gather | solution.py:66
  9.3 341.1 %all-gather.14.cloned.1.call-start = ((), (), s32[]{:S(2)}) async-start(), calls=%async_computation.3 | async-start | bytes 4456448 | tf_op jit(solution)/shard_map/all_gather | solution.py:63
  9.9 413.4 %all-gather.12.cloned.1.call-start = ((), (), s32[]{:S(2)}) async-start(), calls=%async_computation.2 | async-start | bytes 3899392 | tf_op jit(solution)/shard_map/all_gather | solution.py:113
  76.9 62.9 %copy-start.3 = (f32[31,768]{1,0:T(8,128)S(1)}, f32[31,768]{1,0:T(8,128)}, u32[]{:S(2)}) copy-start(f32[31,768]{1,0:T(8,128)} %param.28) | copy-start | bytes 285700
  76.9 419.4 %all-gather.18.cloned.1.call-start = ((), (), s32[]{:S(2)}) async-start(), calls=%async_computation.5 | async-start | bytes 3899392 | tf_op jit(solution)/shard_map/all_gather | solution.py:114
  138.2 461.5 %all-gather.20.cloned.1.call-start = ((), (), s32[]{:S(2)}) async-start(), calls=%async_computation.6 | async-start | bytes 4456448 | tf_op jit(solution)/shard_map/all_gather | solution.py:146
  139.0 503.5 %all-gather.26.cloned.1.call-start = ((), (), s32[]{:S(2)}) async-start(), calls=%async_computation.9 | async-start | bytes 3342336 | tf_op jit(solution)/shard_map/all_gather | solution.py:147
  139.7 513.8 %reduce-scatter.2.cloned.1.call-start = ((), (), s32[]{:S(2)}) async-start(), calls=%async_computation.10 | async-start | bytes 1376256 | tf_op jit(solution)/shard_map/reduce_scatter | solution.py:150
  207.6 73.8 %copy-start.5 = (f32[8]{0:T(128)S(1)}, f32[8]{0:T(128)}, u32[]{:S(2)}) copy-start(f32[8]{0:T(128)} %param.26) | copy-start | bytes 100
  276.6 4.9 collective-permute-start
  280.0 5.7 collective-permute-start.1
  354.2 0.7 copy-start.4
  600.0 42.4 %copy-start.2 = (f32[224,768]{1,0:T(8,128)S(1)}, f32[224,768]{1,0:T(8,128)}, u32[]{:S(2)}) copy-start(f32[224,768]{1,0:T(8,128)} %get-tuple-element.131) | copy-start | bytes 2064388
  600.0 42.4 %copy-start.7 = (f32[768]{0:T(1024)S(1)}, f32[768]{0:T(1024)}, u32[]{:S(2)}) copy-start(f32[768]{0:T(1024)} %param.29) | copy-start | bytes 9220
  642.5 11.1 %copy-start.1 = (f32[128]{0:T(128)S(1)}, f32[128]{0:T(128)}, u32[]{:S(2)}) copy-start(f32[128]{0:T(128)} %param.27) | copy-start | bytes 1540
Sparse Core Ops, SparseCore 0:
  10.1 63.0 all-gather.9
  76.0 59.1 all-gather.15
  138.0 66.6 all-gather.23
  207.3 66.3 all-gather.21
  276.4 74.0 all-gather.13
  353.0 70.2 all-gather.11
  426.0 70.1 all-gather.17
  499.0 74.1 all-gather.19
  575.9 66.4 all-gather.25
  646.7 6.7 reduce-scatter.1
where the time goes:
time: 661 us; the launch traced here: 660 us
  waiting for transfers between devices  502 us (76%)
  matrix products  73.5 us (11%)
  other arithmetic  42.7 us (6%)
  local copies, waits for them, and re-layouts  17.9 us (3%)
  between operations  13.8 us (2%)
    all_gather x1, waiting for transfers between devices, local(): lax.all_gather(value_rows, 'sp', axis=0, tiled=True)  72.9 us
    all_gather x1, waiting for transfers between devices, local(): lax.all_gather(key_rows, 'sp', axis=0, tiled=True)  68.1 us
    all_gather x1, waiting for transfers between devices, local(): lax.all_gather(glu_value_weight, 'sp', axis=0, tiled=True)  66.2 us
    all_gather x1, waiting for transfers between devices, local(): lax.all_gather(glu_gate_weight, 'sp', axis=0, tiled=True)  64.7 us
    all_gather x1, waiting for transfers between devices, local(): lax.all_gather(key_weight, 'sp', axis=0, tiled=True)  59.5 us
    all_gather x1, waiting for transfers between devices, local(): lax.all_gather(value_weight, 'sp', axis=0, tiled=True)  58.3 us
    all_gather x1, waiting for transfers between devices, local(): lax.all_gather(query_weight, 'sp', axis=0, tiled=True)  57.6 us
    all_gather x1, waiting for transfers between devices, local(): lax.all_gather(conv_out_weight, 'sp', axis=0, tiled=True)  38.7 us
  transfers between devices with their start and end apart: 12, of which 10 were waited for; matrix products, arithmetic and copies ran while one was open for 20% of the time, Pallas kernels for 0%

commit v1 on v0

--- a/solution.py
+++ b/solution.py
@@ -1,6 +1,10 @@
+import functools
+
 import jax
 import jax.numpy as jnp
 from jax import lax
+from jax.experimental import pallas as pl
+from jax.experimental.pallas import tpu as pltpu
 from jax.sharding import PartitionSpec as P
 
 HEAD_DIM = 64
@@ -152,9 +156,407 @@
     )
 
 
+PLANE = 4
+RING = 4
+LOG2E = 1.4426950408889634
+
+
+def where_am_i():
+    me = lax.axis_index("sp")
+    core = lax.axis_index("tp")
+    group = me // PLANE
+    spot = me % PLANE
+    along_y = spot // 2
+    along_x = spot % 2
+    x_peer = group * PLANE + along_y * 2 + (1 - along_x)
+    y_peer = group * PLANE + (1 - along_y) * 2 + along_x
+    diagonal = group * PLANE + (1 - along_y) * 2 + (1 - along_x)
+    right = ((group + 1) % RING) * PLANE + spot
+    left = ((group + RING - 1) % RING) * PLANE + spot
+    return core, group, spot, x_peer, y_peer, diagonal, right, left
+
+
+def at(sp, tp):
+    return {"sp": sp, "tp": tp}
+
+
+def greet(peers):
+    barrier = pltpu.get_barrier_semaphore()
+    for peer in peers:
+        pl.semaphore_signal(
+            barrier, inc=1, device_id=peer, device_id_type=pl.DeviceIdType.MESH
+        )
+    pl.semaphore_wait(barrier, len(peers))
+
+
+def send(src, dst, send_sem, recv_sem, peer):
+    copy = pltpu.make_async_remote_copy(
+        src_ref=src,
+        dst_ref=dst,
+        send_sem=send_sem,
+        recv_sem=recv_sem,
+        device_id=peer,
+        device_id_type=pl.DeviceIdType.MESH,
+    )
+    copy.start()
+    return copy
+
+
+def gather_kernel(w_ref, t_ref, wout, tout, own_sem, ws, wr, zs, zr, ts, tr, ps, pr):
+    core, group, spot, x_peer, y_peer, diagonal, right, left = where_am_i()
+    other = 1 - core
+    me = group * PLANE + spot
+    greet(
+        [
+            at(x_peer, core),
+            at(y_peer, core),
+            at(diagonal, core),
+            at(right, core),
+            at(left, core),
+            at(me, other),
+        ]
+    )
+    mine_w = pltpu.make_async_copy(w_ref.at[spot], wout.at[group, spot], own_sem.at[0])
+    mine_w.start()
+    mine_t = pltpu.make_async_copy(t_ref, tout.at[core, spot], own_sem.at[1])
+    mine_t.start()
+    first = []
+    for slot, peer in enumerate((x_peer, y_peer, diagonal)):
+        first.append(
+            send(
+                w_ref.at[peer % PLANE],
+                wout.at[group, spot],
+                ws.at[slot],
+                wr.at[slot],
+                at(peer, core),
+            )
+        )
+    tok = [
+        send(t_ref, tout.at[core, spot], ts.at[0], tr.at[0], at(x_peer, core)),
+        send(t_ref, tout.at[core, spot], ts.at[1], tr.at[1], at(y_peer, core)),
+    ]
+    part = [send(t_ref, tout.at[core, spot], ps.at[0], pr.at[0], at(me, other))]
+    mine_w.wait()
+    for copy in first:
+        copy.wait_recv()
+    ring = [
+        send(wout.at[group], wout.at[group], zs.at[0], zr.at[0], at(right, core)),
+        send(wout.at[group], wout.at[group], zs.at[1], zr.at[1], at(left, core)),
+    ]
+    half = t_ref.shape[0] // 2
+    from_x = x_peer % PLANE
+    from_y = y_peer % PLANE
+    from_d = diagonal % PLANE
+    tok[0].wait_recv()
+    block = tout.at[core, from_x]
+    piece = tout.at[core, from_x, pl.ds(0, half)]
+    tok.append(send(piece, piece, ts.at[2], tr.at[2], at(y_peer, core)))
+    part.append(send(block, block, ps.at[1], pr.at[1], at(me, other)))
+    tok[1].wait_recv()
+    block = tout.at[core, from_y]
+    piece = tout.at[core, from_y, pl.ds(half, half)]
+    tok.append(send(piece, piece, ts.at[3], tr.at[3], at(x_peer, core)))
+    part.append(send(block, block, ps.at[2], pr.at[2], at(me, other)))
+    tok[2].wait_recv()
+    tok[3].wait_recv()
+    block = tout.at[core, from_d]
+    part.append(send(block, block, ps.at[3], pr.at[3], at(me, other)))
+    cut = PLANE // 2
+    from_left = left // PLANE
+    from_right = right // PLANE
+    ring[0].wait_recv()
+    piece = wout.at[from_left, pl.ds(0, cut)]
+    ring.append(send(piece, piece, zs.at[2], zr.at[2], at(right, core)))
+    ring[1].wait_recv()
+    piece = wout.at[from_right, pl.ds(cut, cut)]
+    ring.append(send(piece, piece, zs.at[3], zr.at[3], at(left, core)))
+    for copy in part:
+        copy.wait_recv()
+    ring[2].wait_recv()
+    ring[3].wait_recv()
+    for copy in first + tok + part + ring:
+        copy.wait_send()
+    mine_t.wait()
+
+
+def keys_kernel(kv_ref, edge_ref, kv_out, edge_out, own_sem, zs, zr, es, er):
+    core, group, spot, x_peer, y_peer, diagonal, right, left = where_am_i()
+    greet([at(right, core), at(left, core)])
+    mine = pltpu.make_async_copy(kv_ref, kv_out.at[group], own_sem.at[0])
+    mine.start()
+    edges = [
+        send(edge_ref.at[1], edge_out.at[0], es.at[0], er.at[0], at(right, core)),
+        send(edge_ref.at[0], edge_out.at[1], es.at[1], er.at[1], at(left, core)),
+    ]
+    ring = [
+        send(kv_ref, kv_out.at[group], zs.at[0], zr.at[0], at(right, core)),
+        send(kv_ref, kv_out.at[group], zs.at[1], zr.at[1], at(left, core)),
+    ]
+    half = kv_ref.shape[0] // 2
+    ring[0].wait_recv()
+    piece = kv_out.at[left // PLANE, pl.ds(0, half)]
+    ring.append(send(piece, piece, zs.at[2], zr.at[2], at(right, core)))
+    ring[1].wait_recv()
+    piece = kv_out.at[right // PLANE, pl.ds(half, half)]
+    ring.append(send(piece, piece, zs.at[3], zr.at[3], at(left, core)))
+    mine.wait()
+    ring[2].wait_recv()
+    ring[3].wait_recv()
+    for copy in edges:
+        copy.wait()
+    for copy in ring:
+        copy.wait_send()
+
+
+def squares_kernel(sq_ref, out_ref, own_sem, ss, sr):
+    core, group, spot, x_peer, y_peer, diagonal, right, left = where_am_i()
+    me = group * PLANE + spot
+    other = 1 - core
+    peers = [at(me, other)]
+    for chip in (x_peer, y_peer, diagonal):
+        peers.append(at(chip, core))
+        peers.append(at(chip, other))
+    greet(peers)
+    mine = pltpu.make_async_copy(sq_ref, out_ref.at[spot * 2 + core], own_sem.at[0])
+    mine.start()
+    copies = [
+        send(sq_ref, out_ref.at[spot * 2 + core], ss.at[i], sr.at[i], peer)
+        for i, peer in enumerate(peers)
+    ]
+    mine.wait()
+    for copy in copies:
+        copy.wait()
+
+
+def sum_kernel(p_ref, o_ref, near, mid, far, ns, nr, fs, fr):
+    core, group, spot, x_peer, y_peer, diagonal, right, left = where_am_i()
+    me = group * PLANE + spot
+    other = 1 - core
+    chips = (diagonal, x_peer, y_peer, me)
+    greet([at(me, other)] + [at(chip, core) for chip in chips[:3]])
+    inner = [
+        send(
+            p_ref.at[chip % PLANE, other],
+            near.at[slot],
+            ns.at[slot],
+            nr.at[slot],
+            at(me, other),
+        )
+        for slot, chip in enumerate(chips)
+    ]
+    outer = []
+    for slot, chip in enumerate(chips):
+        inner[slot].wait_recv()
+        total = p_ref[chip % PLANE, core].astype(jnp.float32) + near[slot].astype(jnp.float32)
+        if slot < 3:
+            mid[slot] = total.astype(jnp.bfloat16)
+            outer.append(
+                send(mid.at[slot], far.at[slot], fs.at[slot], fr.at[slot], at(chip, core))
+            )
+    for slot in range(3):
+        outer[slot].wait_recv()
+        total = total + far[slot].astype(jnp.float32)
+    o_ref[...] = total.astype(o_ref.dtype)
+    for copy in inner + outer:
+        copy.wait_send()
+
+
+def attend_kernel(lam_ref, gain_ref, q_ref, kv_ref, o_ref, *, step):
+    width = 2 * HEAD_DIM
+    tall = q_ref.shape[2]
+    ratios = []
+    for pair in range(2):
+        query = q_ref[0, pair]
+        numer = jnp.zeros((tall, width), jnp.float32)
+        sums = jnp.zeros((tall, width), jnp.float32)
+        for start in range(0, kv_ref.shape[0], step):
+            scores = contract_last(query, kv_ref[start : start + step, :width])
+            expo = jnp.exp2(scores * (LOG2E * HEAD_DIM ** (-0.5)))
+            for lane in range(0, step, width):
+                sums = sums + expo[:, lane : lane + width]
+            numer = numer + jnp.dot(
+                expo.astype(jnp.bfloat16),
+                kv_ref[start : start + step, width:],
+                preferred_element_type=jnp.float32,
+            )
+        ratios.append(numer / jnp.sum(sums, axis=1, keepdims=True))
+    rows = ratios[0] - lam_ref[pl.program_id(0)] * ratios[1]
+    o_ref[...] = (rms_scale(rows, gain_ref[...]) * (1.0 - LAMBDA_INIT)).astype(o_ref.dtype)
+
+
+VMEM = pl.BlockSpec(memory_space=pltpu.VMEM)
+DMA = pltpu.SemaphoreType.DMA
+
+
+def exchange(kernel, number, shapes, scratch, *operands):
+    return pl.pallas_call(
+        kernel,
+        out_shape=shapes,
+        in_specs=[VMEM] * len(operands),
+        out_specs=jax.tree.map(lambda _: VMEM, shapes),
+        scratch_shapes=scratch,
+        compiler_params=pltpu.CompilerParams(
+            collective_id=number, has_side_effects=True, vmem_limit_bytes=48 * 2**20
+        ),
+        name=kernel.__name__,
+    )(*operands)
+
+
+def grouped(
+    tokens,
+    norm_gain,
+    query_weight,
+    key_weight,
+    value_weight,
+    glu_value_weight,
+    glu_gate_weight,
+    query_gain,
+    key_gain,
+    lambdas,
+    head_gain,
+    conv_weight,
+    channel_gain,
+    attn_out_weight,
+    conv_out_weight,
+):
+    bf16, f32 = jnp.bfloat16, jnp.float32
+    shape = jax.ShapeDtypeStruct
+    me = lax.axis_index("sp")
+    group, spot = me // PLANE, me % PLANE
+    weights = (
+        query_weight,
+        key_weight,
+        value_weight,
+        attn_out_weight,
+        glu_value_weight,
+        glu_gate_weight,
+        conv_out_weight,
+    )
+    depth = query_weight.shape[0]
+    widths = [w.shape[1] // PLANE for w in weights]
+    packed = jnp.concatenate(
+        [w.reshape(depth, PLANE, n) for w, n in zip(weights, widths)], axis=2
+    ).transpose(1, 0, 2)
+    tok_rows, half_width = tokens.shape
+    w_all, t_all = exchange(
+        gather_kernel,
+        0,
+        (
+            shape((RING, PLANE, depth, packed.shape[2]), bf16),
+            shape((2, PLANE, tok_rows, half_width), bf16),
+        ),
+        [DMA((2,)), DMA((3,)), DMA((3,))] + [DMA((4,))] * 6,
+        packed,
+        tokens,
+    )
+    w_all = w_all.reshape(RING * PLANE * depth, packed.shape[2])
+    rows = PLANE * tok_rows
+    gathered = jnp.concatenate(
+        [t_all[0].reshape(rows, half_width), t_all[1].reshape(rows, half_width)], axis=1
+    ).astype(f32)
+    normed = rms_scale(gathered, norm_gain).astype(bf16)
+    ends = [sum(widths[:i]) for i in range(len(widths) + 1)]
+
+    def project(first, last):
+        return jnp.dot(
+            normed, w_all[:, ends[first] : ends[last]], preferred_element_type=f32
+        )
+
+    width = 2 * HEAD_DIM
+    q_heads = widths[0] // width
+    qkv = project(0, 3)
+    queries = qkv[:, : ends[1]].reshape(rows, q_heads, 2, HEAD_DIM)
+    queries = rms_scale(queries, query_gain).astype(bf16)
+    low = jnp.pad(queries[:, :, 0], ((0, 0), (0, 0), (0, HEAD_DIM)))
+    high = jnp.pad(queries[:, :, 1], ((0, 0), (0, 0), (HEAD_DIM, 0)))
+    queries = jnp.stack([low, high], axis=0).transpose(2, 0, 1, 3)
+    keys = qkv[:, ends[1] : ends[2]].reshape(rows, 2, HEAD_DIM)
+    keys = rms_scale(keys, key_gain).astype(bf16).reshape(rows, width)
+    kv = jnp.concatenate([keys, qkv[:, ends[2] : ends[3]].astype(bf16)], axis=1)
+    glu = project(4, 6)
+    channels = widths[4]
+    glu_rows = (glu[:, :channels] * jax.nn.sigmoid(glu[:, channels:])).astype(bf16)
+    reach = CONV_W // 2
+    border = 16
+    edges = jnp.stack([glu_rows[:border], glu_rows[rows - border :]])
+    kv_all, halo = exchange(
+        keys_kernel,
+        1,
+        (shape((RING, rows, 2 * width), bf16), shape(edges.shape, bf16)),
+        [DMA((1,)), DMA((4,)), DMA((4,)), DMA((2,)), DMA((2,))],
+        kv,
+        edges,
+    )
+    before = jnp.where(group > 0, halo[0], 0)[border - reach :]
+    after = jnp.where(group < RING - 1, halo[1], 0)[:reach]
+    padded = jnp.concatenate([before, glu_rows, after], axis=0).astype(f32)
+    taps = lax.dynamic_slice_in_dim(conv_weight, spot * channels, channels, axis=1)
+    gains = lax.dynamic_slice_in_dim(channel_gain, spot * channels, channels, axis=0)
+    conv_sum = jnp.zeros((rows, channels), f32)
+    for offset in range(CONV_W):
+        conv_sum = conv_sum + taps[offset] * padded[offset : offset + rows]
+    squares = jnp.sum(conv_sum * conv_sum, axis=1).reshape(rows // 128, 128)
+    squares = jnp.pad(squares, ((0, -squares.shape[0] % 8), (0, 0)))
+    shared = exchange(
+        squares_kernel,
+        2,
+        shape((2 * PLANE,) + squares.shape, f32),
+        [DMA((1,)), DMA((7,)), DMA((7,))],
+        squares,
+    )
+    squares = jnp.sum(shared, axis=0).reshape(-1)[:rows]
+    scaled = conv_sum * lax.rsqrt(squares / C_CH + EPS)[:, None] * gains
+    conv_out = jax.nn.silu(scaled).astype(bf16)
+
+    lam = lax.dynamic_slice_in_dim(lambdas, spot * q_heads, q_heads, axis=0)
+    total = RING * rows
+    tall = rows // 2
+    att_out = pl.pallas_call(
+        functools.partial(attend_kernel, step=512),
+        out_shape=shape((rows, q_heads * width), bf16),
+        grid=(q_heads, 2),
+        in_specs=[
+            pl.BlockSpec(memory_space=pltpu.SMEM),
+            pl.BlockSpec((1, width), lambda h, t: (0, 0)),
+            pl.BlockSpec((1, 2, tall, width), lambda h, t: (h, 0, t, 0)),
+            pl.BlockSpec((total, 2 * width), lambda h, t: (0, 0)),
+        ],
+        out_specs=pl.BlockSpec((tall, width), lambda h, t: (t, h)),
+        compiler_params=pltpu.CompilerParams(vmem_limit_bytes=48 * 2**20),
+        name="attend",
+    )(lam, head_gain.reshape(1, width), queries, kv_all.reshape(total, 2 * width))
+
+    mixed = contract_last(att_out, w_all[:, ends[3] : ends[4]]) + contract_last(
+        conv_out, w_all[:, ends[6] : ends[7]]
+    )
+    mixed = mixed.astype(bf16).reshape(PLANE, 2, tok_rows // 2, mixed.shape[1])
+    block = mixed.shape[2:]
+    return exchange(
+        sum_kernel,
+        3,
+        shape(block, bf16),
+        [
+            pltpu.VMEM((4,) + block, bf16),
+            pltpu.VMEM((3,) + block, bf16),
+            pltpu.VMEM((3,) + block, bf16),
+            DMA((4,)),
+            DMA((4,)),
+            DMA((3,)),
+            DMA((3,)),
+        ],
+        mixed,
+    )
+
+
+def body_for(mesh):
+    if mesh.shape["sp"] == RING * PLANE and mesh.shape["tp"] == 2:
+        return grouped
+    return local
+
+
 def solution(mesh):
     return jax.shard_map(
-        local,
+        body_for(mesh),
         mesh=mesh,
         in_specs=(
             P("sp", "tp"),

time: 661 us -> 238 us (0.36)
  waiting for transfers between devices: 502 us -> 0 us
  Pallas kernels: 0 us -> 200 us
  matrix products: 73.5 us -> 9.51 us
  other arithmetic: 42.7 us -> 7.29 us
  between operations: 13.8 us -> 0.71 us
    all_gather x9 -> x0, waiting for transfers between devices: 486 us -> none  [the longest x1 72.9 us: local(): lax.all_gather(value_rows, 'sp', axis=0, tiled=True)]
    pallas_call x0 -> x5, Pallas kernels: none -> 200 us  [the longest x4 182 us: exchange(): pl.pallas_call(kernel, out_shape=shapes, in_specs=[VMEM] * len(operands),...]
    dot_general x13 -> x2, matrix products: 65.7 us -> 4.71 us  [project(): jnp.dot(normed, w_all[:, ends[first]:ends[last]], preferred_element_type=...]
    convert_element_type x5 -> x4, other arithmetic: 34.8 us -> 2.27 us  [the longest x1 1.2 us: grouped(): queries = rms_scale(queries, query_gain).astype(bf16)]
    unnamed x17 -> x56, local copies, waits for them, and re-layouts: 0.24 us -> 9.23 us
    dynamic_slice x12 -> x2, local copies, waits for them, and re-layouts: 11.1 us -> 2.12 us  [the longest x1 1.34 us: grouped(): lax.dynamic_slice_in_dim(channel_gain, spot * channels, channels, axis=0)]
    reduce_scatter x1 -> x0, waiting for transfers between devices: 6.95 us -> none  [local(): lax.psum_scatter(partial_term.astype(jnp.bfloat16), 'tp', scatter_dimensi...]
  transfers between devices with their start and end apart: 12 -> 0, of which waited for: 10 -> 0; matrix products, arithmetic and copies ran while one was open for 20% -> 0% of each run, Pallas kernels for 0% -> 0%
where the time goes in v1:
time: 238 us; the launch traced here: 237 us
  Pallas kernels  200 us (84%)
  local copies, waits for them, and re-layouts  20.4 us (9%)
  matrix products  9.51 us (4%)
  other arithmetic  7.29 us (3%)
    pallas_call x4, Pallas kernels, exchange(): pl.pallas_call(kernel, out_shape=shapes, in_specs=[VMEM] * len(operands),...  182 us
    pallas_call x1, Pallas kernels, grouped(): pl.pallas_call(functools.partial(attend_kernel, step=512), out_shape=shap...  17.1 us
    unnamed x56, local copies, waits for them, and re-layouts  9.23 us
    dot_general x2, matrix products, contract_last(): lax.dot_general(left, right, (((1,), (1,)), ((), ())), preferred_element_...  4.8 us

profile of v1, /device:TPU:0, one launch (start us, length us, event | category | flops | bytes accessed | tf_op | source)
XLA Modules:
  0.0 237.5 jit_solution(7337368840386872642)
XLA Ops:
  0.0 0.8 dynamic_slice.9.lam_ref
  0.8 0.7 mul.427
  1.4 0.6 mul.428
  2.0 1.3 dynamic_slice.11
  3.3 1.1 fusion.55
  4.5 2.0 constant_dynamic-slice_fusion
  6.5 1.0 copy.44
  7.5 0.1 copy.51
  7.6 1.0 copy.45
  8.7 0.1 copy.52
  8.8 1.1 copy.47
  9.9 0.1 copy.54
  10.1 1.1 copy.48
  11.2 0.2 copy.55
  11.3 1.1 copy.49
  12.4 0.2 copy.56
  12.6 0.2 copy.43
  12.8 0.2 copy.50
  13.0 0.2 copy.46
  13.1 0.2 copy.53
  13.3 2.0 concatenate.12
  15.3 119.7 %gather_kernel.1 = (bf16[4,4,128,1344]{3,2,1,0:T(8,128)(2,1)}, bf16[2,4,224,1024]{3,2,1,0:T(8,128)(2,1)S(1)}) custom-call(bf16[4,128,1344]{2,1,0:T(8,128)(2,1)S(1)} %bitcast.75, bf16[224,1024]{1,0:T(8,128)(2,1)S(1)} %copy-done), custom_call_target="tpu_custom_call" | custom-call | tf_op jit(solution)/shard_map/gather_kernel/pallas_call | solution.py:392
  135.1 0.4 fusion.54
  135.5 0.8 fusion
  136.3 0.9 slice-done.1
  137.2 0.5 slice-done.2
  137.7 2.1 fusion.5
  139.9 2.6 %fusion.3 = f32[896,512]{0,1:T(8,128)S(1)} fusion(bf16[2048,1344]{1,0:T(8,128)(2,1)S(1)} %bitcast.96, f32[2048]{0:T(1024)S(1)} %copy-done.20, f32[896]{0:T(1024)S(1)} %add_rsqrt_fusion.2, bf16[896,1024]{1,0:T(8,128)(2,1)S(1)} %bitcast.83, bf16[896,1024]{1,0:T(8,128)(2,1)S(1)} %bitcast.80), kind=kOutput, calls=%fused_computation.7 | convolution fusion | flops 1891893248 | bytes 7614464 | tf_op jit(solution)/shard_map/dot_general | solution.py:461
  142.5 0.3 fusion.44
  142.8 0.1 multiply_reduce_fusion.1
  143.0 0.9 copy-done.3
  143.9 0.2 copy.68
  144.1 0.2 copy.67
  144.4 0.2 copy.61
  144.7 0.2 copy.62
  144.9 0.6 multiply_convert_fusion.3
  145.6 0.5 copy.58
  146.1 1.2 multiply_convert_fusion
  147.4 0.2 pad_bitcast_fusion
  147.9 32.3 %keys_kernel.1 = (bf16[4,896,256]{2,1,0:T(8,128)(2,1)S(1)}, bf16[2,16,192]{2,1,0:T(8,128)(2,1)S(1)}) custom-call(bf16[896,256]{1,0:T(8,128)(2,1)S(1)} %pad_maximum_fusion.1.kv_ref, bf16[2,16,192]{2,1,0:T(8,128)(2,1)S(1)} %pad_maximum_fusion.2.edge_ref), custom_call_target="tpu_custom_call" | custom-call | tf_op jit(solution)/shard_map/keys_kernel/pallas_call | solution.py:392
  180.2 17.1 %attend.1 = bf16[896,256]{1,0:T(8,128)(2,1)S(1)} custom-call(f32[2]{0:T(128)S(1)} %dynamic_slice.9.lam_ref, f32[1,128]{1,0:T(1,128)S(1)} %bitcast.77, bf16[2,2,896,128]{3,2,1,0:T(8,128)(2,1)S(1)} %maximum_bitcast_fusion.q_ref, bf16[3584,256]{1,0:T(8,128)(2,1)S(1)} %bitcast.76), custom_call_target="tpu_custom_call" | custom-call | tf_op jit(solution)/shard_map/attend/pallas_call | solution.py:514
  197.4 0.1 maximum_convert_fusion
  197.6 3.8 %multiply_reduce_fusion = (f32[896]{0:T(1024)S(1)}, f32[896,192]{1,0:T(8,128)S(1)}) fusion(f32[926,192]{1,0:T(8,128)S(1)} %maximum_convert_fusion, f32[192]{0:T(256)S(1)} %bitcast.112, f32[192]{0:T(256)S(1)} %bitcast.114, f32[192]{0:T(256)S(1)} %bitcast.115, f32[192]{0:T(256)S(1)} %bitcast.116, f32[192]{0:T(256)S(1)} %bitcast.117, f32[192]{0:T(256)S(1)} %bitcast.118, ...), kind=kLoop, calls=%fused_computation.83 | loop fusion | flops 10837120 | bytes 22047488 | tf_op jit(solution)/shard_map/reduce_sum | solution.py:498
  201.4 4.8 %squares_kernel.1 = f32[8,8,128]{2,1,0:T(8,128)S(1)} custom-call(f32[8,128]{1,0:T(8,128)S(1)} %pad.14.sq_ref), custom_call_target="tpu_custom_call" | custom-call | tf_op jit(solution)/shard_map/squares_kernel/pallas_call | solution.py:392
  206.3 2.4 %fusion.8 = f32[896,2048]{1,0:T(8,128)S(1)} fusion(bf16[896,256]{1,0:T(8,128)(2,1)S(1)} %attend.1, bf16[2048,1344]{1,0:T(8,128)(2,1)} %bitcast.91), kind=kOutput, calls=%fused_computation.13 | convolution fusion | flops 939524096 | bytes 8847360 | tf_op jit(solution)/shard_map/dot_general | solution.py:41
  208.7 2.4 %add_convert_fusion = bf16[896,2048]{1,0:T(8,128)(2,1)S(1)} fusion(f32[896,2048]{1,0:T(8,128)S(1)} %fusion.8, bf16[2048,1344]{1,0:T(8,128)(2,1)} %bitcast.92, f32[896,192]{1,0:T(8,128)S(1)} %get-tuple-element.14, f32[192]{0:T(256)S(1)} %copy-done.19, f32[896]{0:T(1024)S(1)} %rsqrt_bitcast_fusion), kind=kOutput, calls=%fused_computation.5 | convolution fusion | flops 709517312 | bytes 12751104 | tf_op jit(solution)/shard_map/dot_general | solution.py:41
  211.1 25.6 %sum_kernel.1 = bf16[112,2048]{1,0:T(8,128)(2,1)S(1)} custom-call(bf16[4,2,112,2048]{3,2,1,0:T(8,128)(2,1)S(1)} %bitcast.74), custom_call_target="tpu_custom_call" | custom-call | tf_op jit(solution)/shard_map/sum_kernel/pallas_call | solution.py:392
  236.7 0.8 copy.70
  (65 shorter events, 0.6 us)
Async XLA Ops:
  0.0 13.0 %copy-start.6 = (bf16[128,1024]{1,0:T(8,128)(2,1)S(1)}, bf16[128,1024]{1,0:T(8,128)(2,1)}, u32[]{:S(2)}) copy-start(bf16[128,1024]{1,0:T(8,128)(2,1)} %param.28) | copy-start | bytes 786436
  0.0 12.6 %copy-start.5 = (bf16[128,1024]{1,0:T(8,128)(2,1)S(1)}, bf16[128,1024]{1,0:T(8,128)(2,1)}, u32[]{:S(2)}) copy-start(bf16[128,1024]{1,0:T(8,128)(2,1)} %param.17) | copy-start | bytes 786436
  9.9 5.4 %copy-start = (bf16[224,1024]{1,0:T(8,128)(2,1)S(1)}, bf16[224,1024]{1,0:T(8,128)(2,1)}, u32[]{:S(2)}) copy-start(bf16[224,1024]{1,0:T(8,128)(2,1)} %t_ref.1) | copy-start | bytes 1376260
  135.1 2.2 slice-start.1
  135.1 2.7 %slice-start.2 = ((s8[5767168]{0:T(1024)(128)(4,1)}), s8[1572864]{0:T(1024)(128)(4,1)S(1)}, s32[]{:S(2)}) async-start(s8[5767168]{0:T(1024)(128)(4,1)} %bitcast.93), calls=%async_computation.2 | async-start | bytes 3145728
  135.5 2.2 copy-start.20
  142.4 1.8 copy-start.2
  142.8 1.0 copy-start.3
  144.3 1.3 slice-start
  147.3 32.8 %copy-start.1 = (f32[128]{0:T(128)S(1)}, f32[128]{0:T(128)}, u32[]{:S(2)}) copy-start(f32[128]{0:T(128)} %param.25) | copy-start | bytes 1540
  147.4 49.9 %copy-start.4 = (bf16[896,192]{1,0:T(8,128)(2,1)S(1)}, bf16[896,192]{1,0:T(8,128)(2,1)}, u32[]{:S(2)}) copy-start(bf16[896,192]{1,0:T(8,128)(2,1)} %copy-done.3) | copy-start | bytes 1032196
  147.7 49.8 %copy-start.7 = (f32[1,192]{1,0:T(1,128)S(1)}, f32[1,192]{1,0:T(1,128)}, u32[]{:S(2)}) copy-start(f32[1,192]{1,0:T(1,128)} %get-tuple-element.27) | copy-start | bytes 2308
  147.7 49.8 %copy-start.8 = (f32[1,192]{1,0:T(1,128)S(1)}, f32[1,192]{1,0:T(1,128)}, u32[]{:S(2)}) copy-start(f32[1,192]{1,0:T(1,128)} %get-tuple-element.28) | copy-start | bytes 2308
  147.7 49.8 %copy-start.9 = (f32[1,192]{1,0:T(1,128)S(1)}, f32[1,192]{1,0:T(1,128)}, u32[]{:S(2)}) copy-start(f32[1,192]{1,0:T(1,128)} %get-tuple-element.29) | copy-start | bytes 2308
  147.7 49.8 %copy-start.10 = (f32[1,192]{1,0:T(1,128)S(1)}, f32[1,192]{1,0:T(1,128)}, u32[]{:S(2)}) copy-start(f32[1,192]{1,0:T(1,128)} %get-tuple-element.30) | copy-start | bytes 2308
  147.7 49.8 %copy-start.11 = (f32[1,192]{1,0:T(1,128)S(1)}, f32[1,192]{1,0:T(1,128)}, u32[]{:S(2)}) copy-start(f32[1,192]{1,0:T(1,128)} %get-tuple-element.31) | copy-start | bytes 2308
  147.7 49.8 %copy-start.12 = (f32[1,192]{1,0:T(1,128)S(1)}, f32[1,192]{1,0:T(1,128)}, u32[]{:S(2)}) copy-start(f32[1,192]{1,0:T(1,128)} %get-tuple-element.32) | copy-start | bytes 2308
  147.7 49.8 %copy-start.13 = (f32[1,192]{1,0:T(1,128)S(1)}, f32[1,192]{1,0:T(1,128)}, u32[]{:S(2)}) copy-start(f32[1,192]{1,0:T(1,128)} %get-tuple-element.33) | copy-start | bytes 2308
  147.7 49.8 %copy-start.14 = (f32[1,192]{1,0:T(1,128)S(1)}, f32[1,192]{1,0:T(1,128)}, u32[]{:S(2)}) copy-start(f32[1,192]{1,0:T(1,128)} %get-tuple-element.34) | copy-start | bytes 2308
  147.8 49.8 %copy-start.15 = (f32[1,192]{1,0:T(1,128)S(1)}, f32[1,192]{1,0:T(1,128)}, u32[]{:S(2)}) copy-start(f32[1,192]{1,0:T(1,128)} %get-tuple-element.35) | copy-start | bytes 2308
  147.8 49.8 %copy-start.16 = (f32[1,192]{1,0:T(1,128)S(1)}, f32[1,192]{1,0:T(1,128)}, u32[]{:S(2)}) copy-start(f32[1,192]{1,0:T(1,128)} %get-tuple-element.36) | copy-start | bytes 2308
  147.8 49.8 %copy-start.17 = (f32[1,192]{1,0:T(1,128)S(1)}, f32[1,192]{1,0:T(1,128)}, u32[]{:S(2)}) copy-start(f32[1,192]{1,0:T(1,128)} %get-tuple-element.37) | copy-start | bytes 2308
  147.8 49.8 %copy-start.18 = (f32[1,192]{1,0:T(1,128)S(1)}, f32[1,192]{1,0:T(1,128)}, u32[]{:S(2)}) copy-start(f32[1,192]{1,0:T(1,128)} %get-tuple-element.38) | copy-start | bytes 2308
  206.3 2.4 %copy-start.19 = (f32[192]{0:T(256)S(1)}, f32[192]{0:T(256)}, u32[]{:S(2)}) copy-start(f32[192]{0:T(256)} %dynamic_slice.11) | copy-start | bytes 2308

commit v2 on v0

--- a/solution.py
+++ b/solution.py
@@ -1,6 +1,8 @@
 import jax
 import jax.numpy as jnp
 from jax import lax
+from jax.experimental import pallas as pl
+from jax.experimental.pallas import tpu as pltpu
 from jax.sharding import PartitionSpec as P
 
 HEAD_DIM = 64
@@ -152,9 +154,556 @@
     )
 
 
+PLANE = 4
+RING = 4
+LOG2E = 1.4426950408889634
+
+
+def where_am_i():
+    me = lax.axis_index("sp")
+    core = lax.axis_index("tp")
+    group = me // PLANE
+    spot = me % PLANE
+    along_y = spot // 2
+    along_x = spot % 2
+    base = group * PLANE
+    x_peer = base + along_y * 2 + (1 - along_x)
+    y_peer = base + (1 - along_y) * 2 + along_x
+    diagonal = base + (1 - along_y) * 2 + (1 - along_x)
+    line = [((group + hop) % RING) * PLANE + spot for hop in range(1, RING)]
+    return core, group, spot, x_peer, y_peer, diagonal, line
+
+
+def at(sp, tp):
+    return {"sp": sp, "tp": tp}
+
+
+def greet(peers):
+    barrier = pltpu.get_barrier_semaphore()
+    for peer in peers:
+        pl.semaphore_signal(
+            barrier, inc=1, device_id=peer, device_id_type=pl.DeviceIdType.MESH
+        )
+    pl.semaphore_wait(barrier, len(peers))
+
+
+def send(src, dst, send_sem, recv_sem, peer):
+    copy = pltpu.make_async_remote_copy(
+        src_ref=src,
+        dst_ref=dst,
+        send_sem=send_sem,
+        recv_sem=recv_sem,
+        device_id=peer,
+        device_id_type=pl.DeviceIdType.MESH,
+    )
+    copy.start()
+    return copy
+
+
+def gather_kernel(
+    q_ref, k_ref, v_ref, g_ref, t_ref, wout, tout, own, ws, wr, xs, xr, us, ur, ds, dr, ps, pr
+):
+    core, group, spot, x_peer, y_peer, diagonal, line = where_am_i()
+    other = 1 - core
+    me = group * PLANE + spot
+    greet(
+        [at(chip, core) for chip in line]
+        + [at(x_peer, core), at(y_peer, core), at(me, other)]
+    )
+
+    def segments(quarter):
+        start = 0
+        for ref in (q_ref, k_ref, v_ref, g_ref):
+            if ref is g_ref:
+                width = ref.shape[2]
+                piece = ref.at[quarter]
+            else:
+                width = ref.shape[1] // RING
+                piece = ref.at[:, pl.ds(pl.multiple_of(quarter * width, width), width)]
+            yield piece, wout.at[group, spot, :, pl.ds(start, width)]
+            start += width
+
+    local_copies = [
+        pltpu.make_async_copy(piece, place, own.at[i])
+        for i, (piece, place) in enumerate(segments(group))
+    ]
+    local_copies.append(pltpu.make_async_copy(t_ref, tout.at[core, group], own.at[4]))
+    for copy in local_copies:
+        copy.start()
+    first = []
+    for hop, chip in enumerate(line):
+        for i, (piece, place) in enumerate(segments(chip // PLANE)):
+            first.append(
+                send(piece, place, ws.at[hop * 4 + i], wr.at[hop * 4 + i], at(chip, core))
+            )
+
+    def token_copy(step, upward):
+        move = 1 if upward else RING - 1
+        source = (group + RING - step * move) % RING
+        target = ((group + move) % RING) * PLANE + spot
+        block = tout.at[core, source]
+        sems = (us, ur) if upward else (ds, dr)
+        return pltpu.make_async_remote_copy(
+            src_ref=t_ref if step == 0 else block,
+            dst_ref=block,
+            send_sem=sems[0].at[step],
+            recv_sem=sems[1].at[step],
+            device_id=at(target, core),
+            device_id_type=pl.DeviceIdType.MESH,
+        )
+
+    def partner_copy(hop):
+        block = tout.at[core, (group + hop) % RING]
+        return pltpu.make_async_remote_copy(
+            src_ref=t_ref if hop == 0 else block,
+            dst_ref=block,
+            send_sem=ps.at[hop],
+            recv_sem=pr.at[hop],
+            device_id=at(me, other),
+            device_id_type=pl.DeviceIdType.MESH,
+        )
+
+    def sends(step, upward):
+        if upward:
+            return jnp.logical_and(group >= step, group < RING - 1)
+        return jnp.logical_and(group < RING - step, group > 0)
+
+    def receives(step, upward):
+        return group > step if upward else group < RING - 1 - step
+
+    partner_copy(0).start()
+    for upward in (True, False):
+
+        @pl.when(sends(0, upward))
+        def _():
+            token_copy(0, upward).start()
+
+    for copy in local_copies:
+        copy.wait()
+    for copy in first:
+        copy.wait_recv()
+    mine = wout.at[:, spot]
+    ring = [
+        send(mine, mine, xs.at[0], xr.at[0], at(x_peer, core)),
+        send(mine, mine, xs.at[1], xr.at[1], at(y_peer, core)),
+    ]
+    for step in range(RING - 1):
+        for upward in (True, False):
+
+            @pl.when(receives(step, upward))
+            def _():
+                token_copy(step, upward).wait_recv()
+                partner_copy(RING - 1 - step if upward else step + 1).start()
+
+            if step < RING - 2:
+
+                @pl.when(sends(step + 1, upward))
+                def _():
+                    token_copy(step + 1, upward).start()
+
+    cut = RING // 2
+    ring[0].wait_recv()
+    piece = wout.at[pl.ds(0, cut), x_peer % PLANE]
+    ring.append(send(piece, piece, xs.at[2], xr.at[2], at(y_peer, core)))
+    ring[1].wait_recv()
+    piece = wout.at[pl.ds(cut, cut), y_peer % PLANE]
+    ring.append(send(piece, piece, xs.at[3], xr.at[3], at(x_peer, core)))
+    for hop in range(RING):
+        partner_copy(hop).wait()
+    for step in range(RING - 1):
+        for upward in (True, False):
+
+            @pl.when(sends(step, upward))
+            def _():
+                token_copy(step, upward).wait_send()
+
+    ring[2].wait_recv()
+    ring[3].wait_recv()
+    for copy in first + ring:
+        copy.wait_send()
+
+
+def squares_kernel(sq_ref, out_ref, own_sem, ss, sr):
+    core, group, spot, x_peer, y_peer, diagonal, line = where_am_i()
+    me = group * PLANE + spot
+    other = 1 - core
+    peers = [at(me, other)]
+    for chip in line:
+        peers.append(at(chip, core))
+        peers.append(at(chip, other))
+    greet(peers)
+    mine = pltpu.make_async_copy(sq_ref, out_ref.at[group * 2 + core], own_sem.at[0])
+    mine.start()
+    copies = [
+        send(sq_ref, out_ref.at[group * 2 + core], ss.at[i], sr.at[i], peer)
+        for i, peer in enumerate(peers)
+    ]
+    mine.wait()
+    for copy in copies:
+        copy.wait()
+
+
+def sum_kernel(p_ref, o_ref, near, mid, far, ns, nr, fs, fr):
+    core, group, spot, x_peer, y_peer, diagonal, line = where_am_i()
+    me = group * PLANE + spot
+    other = 1 - core
+    chips = [line[1], line[0], line[2], me]
+    greet([at(me, other)] + [at(chip, core) for chip in chips[:3]])
+    inner = [
+        send(
+            p_ref.at[chip // PLANE, other],
+            near.at[slot],
+            ns.at[slot],
+            nr.at[slot],
+            at(me, other),
+        )
+        for slot, chip in enumerate(chips)
+    ]
+    outer = []
+    for slot, chip in enumerate(chips):
+        inner[slot].wait_recv()
+        total = p_ref[chip // PLANE, core].astype(jnp.float32) + near[slot].astype(jnp.float32)
+        if slot < 3:
+            mid[slot] = total.astype(jnp.bfloat16)
+            outer.append(
+                send(mid.at[slot], far.at[slot], fs.at[slot], fr.at[slot], at(chip, core))
+            )
+    for slot in range(3):
+        outer[slot].wait_recv()
+        total = total + far[slot].astype(jnp.float32)
+    o_ref[...] = total.astype(o_ref.dtype)
+    for copy in inner + outer:
+        copy.wait_send()
+
+
+def attend_kernel(
+    lam_ref, gain_ref, q_ref, kv_ref, edge_ref, a_ref, c_ref,
+    o_ref, edge_out, a_out, c_out,
+    kv_all, numer, sums, own, es, er, zs, zr, ws, wr, xs, xr,
+):
+    core, group, spot, x_peer, y_peer, diagonal, line = where_am_i()
+    greet(
+        [at(x_peer, core), at(y_peer, core), at(diagonal, core)]
+        + [at(chip, core) for chip in line]
+    )
+    keys = [
+        send(kv_ref, kv_all.at[0], zs.at[0], zr.at[0], at(x_peer, core)),
+        send(kv_ref, kv_all.at[1], zs.at[1], zr.at[1], at(y_peer, core)),
+    ]
+    base = group * PLANE
+    after = base + (spot + 1) % PLANE
+    before = base + (spot + PLANE - 1) % PLANE
+    edges = [
+        send(edge_ref.at[1], edge_out.at[0], es.at[0], er.at[0], at(after, core)),
+        send(edge_ref.at[0], edge_out.at[1], es.at[1], er.at[1], at(before, core)),
+    ]
+
+    def columns(quarter):
+        width = a_ref.shape[1] // RING
+        return a_ref.at[:, pl.ds(pl.multiple_of(quarter * width, width), width)]
+
+    mine = [
+        pltpu.make_async_copy(columns(group), a_out.at[group, spot], own.at[0]),
+        pltpu.make_async_copy(c_ref.at[group], c_out.at[group, spot], own.at[1]),
+    ]
+    for copy in mine:
+        copy.start()
+    first = []
+    for hop, chip in enumerate(line):
+        peer = at(chip, core)
+        first.append(
+            send(columns(chip // PLANE), a_out.at[group, spot], ws.at[hop], wr.at[hop], peer)
+        )
+        first.append(
+            send(
+                c_ref.at[chip // PLANE],
+                c_out.at[group, spot],
+                ws.at[3 + hop],
+                wr.at[3 + hop],
+                peer,
+            )
+        )
+
+    width = 2 * HEAD_DIM
+    rows = q_ref.shape[1]
+    tall = rows // 2
+    count = kv_ref.shape[0]
+    step = 512
+
+    def attend(block, fresh):
+        @pl.loop(0, q_ref.shape[0] * 2)
+        def _(turn):
+            lead = turn // 2
+            span = pl.ds(pl.multiple_of((turn % 2) * tall, tall), tall)
+            query = q_ref[lead, span]
+            if fresh:
+                total = jnp.zeros((tall, width), jnp.float32)
+                weighted = jnp.zeros((tall, width), jnp.float32)
+            else:
+                total = sums[lead, span]
+                weighted = numer[lead, span]
+            for start in range(0, count, step):
+                stop = min(start + step, count)
+                scores = contract_last(query, block[start:stop, :width])
+                expo = jnp.exp2(scores * (LOG2E * HEAD_DIM ** (-0.5)))
+                for lane in range(0, stop - start, width):
+                    total = total + expo[:, lane : lane + width]
+                weighted = weighted + jnp.dot(
+                    expo.astype(jnp.bfloat16),
+                    block[start:stop, width:],
+                    preferred_element_type=jnp.float32,
+                )
+            sums[lead, span] = total
+            numer[lead, span] = weighted
+
+    attend(kv_ref, True)
+    half = count // 2
+    keys[0].wait_recv()
+    keys.append(
+        send(
+            kv_all.at[0, pl.ds(0, half)],
+            kv_all.at[2, pl.ds(0, half)],
+            zs.at[2],
+            zr.at[2],
+            at(y_peer, core),
+        )
+    )
+    keys[1].wait_recv()
+    keys.append(
+        send(
+            kv_all.at[1, pl.ds(half, half)],
+            kv_all.at[2, pl.ds(half, half)],
+            zs.at[3],
+            zr.at[3],
+            at(x_peer, core),
+        )
+    )
+    for copy in mine:
+        copy.wait()
+    for copy in first:
+        copy.wait_recv()
+    ring = []
+    for i, buf in enumerate((a_out, c_out)):
+        block = buf.at[:, spot]
+        ring.append(send(block, block, xs.at[i], xr.at[i], at(x_peer, core)))
+        ring.append(send(block, block, xs.at[2 + i], xr.at[2 + i], at(y_peer, core)))
+    attend(kv_all.at[0], False)
+    attend(kv_all.at[1], False)
+    cut = RING // 2
+    for i, buf in enumerate((a_out, c_out)):
+        ring[2 * i].wait_recv()
+        piece = buf.at[pl.ds(0, cut), x_peer % PLANE]
+        ring.append(send(piece, piece, xs.at[4 + i], xr.at[4 + i], at(y_peer, core)))
+        ring[2 * i + 1].wait_recv()
+        piece = buf.at[pl.ds(cut, cut), y_peer % PLANE]
+        ring.append(send(piece, piece, xs.at[6 + i], xr.at[6 + i], at(x_peer, core)))
+    keys[2].wait_recv()
+    keys[3].wait_recv()
+    attend(kv_all.at[2], False)
+    for head in range(q_ref.shape[0] // 2):
+
+        @pl.loop(0, 2)
+        def _(turn):
+            span = pl.ds(pl.multiple_of(turn * tall, tall), tall)
+            ratios = [
+                numer[2 * head + pair, span]
+                / jnp.sum(sums[2 * head + pair, span], axis=1, keepdims=True)
+                for pair in range(2)
+            ]
+            att = ratios[0] - lam_ref[head] * ratios[1]
+            att = rms_scale(att, gain_ref[...]) * (1.0 - LAMBDA_INIT)
+            o_ref[span, head * width : (head + 1) * width] = att.astype(o_ref.dtype)
+
+    for copy in ring[4:]:
+        copy.wait_recv()
+    for copy in edges:
+        copy.wait()
+    for copy in keys + first + ring:
+        copy.wait_send()
+
+
+VMEM = pl.BlockSpec(memory_space=pltpu.VMEM)
+DMA = pltpu.SemaphoreType.DMA
+
+
+def exchange(kernel, number, shapes, scratch, *operands, scalars=0):
+    return pl.pallas_call(
+        kernel,
+        out_shape=shapes,
+        in_specs=[pl.BlockSpec(memory_space=pltpu.SMEM)] * scalars
+        + [VMEM] * (len(operands) - scalars),
+        out_specs=jax.tree.map(lambda _: VMEM, shapes),
+        scratch_shapes=scratch,
+        compiler_params=pltpu.CompilerParams(
+            collective_id=number, has_side_effects=True, vmem_limit_bytes=56 * 2**20
+        ),
+        name=kernel.__name__,
+    )(*operands)
+
+
+def grouped(
+    tokens,
+    norm_gain,
+    query_weight,
+    key_weight,
+    value_weight,
+    glu_value_weight,
+    glu_gate_weight,
+    query_gain,
+    key_gain,
+    lambdas,
+    head_gain,
+    conv_weight,
+    channel_gain,
+    attn_out_weight,
+    conv_out_weight,
+):
+    bf16, f32 = jnp.bfloat16, jnp.float32
+    shape = jax.ShapeDtypeStruct
+    me = lax.axis_index("sp")
+    group, spot = me // PLANE, me % PLANE
+    depth = query_weight.shape[0]
+    width = 2 * HEAD_DIM
+    q_cols = query_weight.shape[1] // RING
+    k_cols = key_weight.shape[1] // RING
+    channels = glu_value_weight.shape[1] // RING
+    q_heads = q_cols // width
+
+    def quarters(*arrays):
+        cut = [a.reshape(a.shape[0], RING, a.shape[1] // RING) for a in arrays]
+        return jnp.concatenate(cut, axis=2).transpose(1, 0, 2)
+
+    tok_rows, half_width = tokens.shape
+    columns = q_cols + 2 * k_cols + 2 * channels
+    w_all, t_all = exchange(
+        gather_kernel,
+        0,
+        (
+            shape((RING, PLANE, depth, columns), bf16),
+            shape((2, RING, tok_rows, half_width), bf16),
+        ),
+        [DMA((5,)), DMA((12,)), DMA((12,)), DMA((4,)), DMA((4,))]
+        + [DMA((3,))] * 4
+        + [DMA((4,))] * 2,
+        query_weight,
+        key_weight,
+        value_weight,
+        quarters(glu_value_weight, glu_gate_weight),
+        tokens,
+    )
+    w_all = w_all.reshape(RING * PLANE * depth, columns)
+    rows = RING * tok_rows
+    gathered = jnp.concatenate(
+        [t_all[0].reshape(rows, half_width), t_all[1].reshape(rows, half_width)], axis=1
+    ).astype(f32)
+    normed = rms_scale(gathered, norm_gain).astype(bf16)
+    qkv_cols = q_cols + 2 * k_cols
+    qkv = jnp.dot(normed, w_all[:, :qkv_cols], preferred_element_type=f32)
+    glu = jnp.dot(normed, w_all[:, qkv_cols:], preferred_element_type=f32)
+    queries = qkv[:, :q_cols].reshape(rows, q_heads, 2, HEAD_DIM)
+    queries = rms_scale(queries, query_gain).astype(bf16)
+    low = jnp.pad(queries[:, :, 0], ((0, 0), (0, 0), (0, HEAD_DIM)))
+    high = jnp.pad(queries[:, :, 1], ((0, 0), (0, 0), (HEAD_DIM, 0)))
+    queries = jnp.stack([low, high], axis=0).transpose(2, 0, 1, 3)
+    queries = queries.reshape(q_heads * 2, rows, width)
+    keys = qkv[:, q_cols : q_cols + k_cols].reshape(rows, 2, HEAD_DIM)
+    keys = rms_scale(keys, key_gain).astype(bf16).reshape(rows, width)
+    kv = jnp.concatenate([keys, qkv[:, q_cols + k_cols :].astype(bf16)], axis=1)
+    glu_rows = (glu[:, :channels] * jax.nn.sigmoid(glu[:, channels:])).astype(bf16)
+    glu_rows = glu_rows.reshape(RING, tok_rows, channels)
+    reach = CONV_W // 2
+    border = 16
+    edges = jnp.stack([glu_rows[:, :border], glu_rows[:, tok_rows - border :]])
+    lam = lax.dynamic_slice_in_dim(lambdas, group * q_heads, q_heads, axis=0)
+    att_out, halo, attn_all, conv_all = exchange(
+        attend_kernel,
+        1,
+        (
+            shape((rows, q_cols), bf16),
+            shape(edges.shape, bf16),
+            shape((RING, PLANE, depth, q_cols), bf16),
+            shape((RING, PLANE, depth, channels), bf16),
+        ),
+        [
+            pltpu.VMEM((3, rows, 2 * width), bf16),
+            pltpu.VMEM((q_heads * 2, rows, width), f32),
+            pltpu.VMEM((q_heads * 2, rows, width), f32),
+            DMA((2,)),
+            DMA((2,)),
+            DMA((2,)),
+            DMA((4,)),
+            DMA((4,)),
+            DMA((6,)),
+            DMA((6,)),
+            DMA((8,)),
+            DMA((8,)),
+        ],
+        lam,
+        head_gain.reshape(1, width),
+        queries,
+        kv,
+        edges,
+        attn_out_weight,
+        quarters(conv_out_weight),
+        scalars=1,
+    )
+    blank = jnp.zeros_like(halo[0, :1])
+    tails = jnp.where(spot > 0, halo[0], jnp.concatenate([blank, halo[0, :-1]]))
+    heads = jnp.where(spot < PLANE - 1, halo[1], jnp.concatenate([halo[1, 1:], blank]))
+    padded = jnp.concatenate(
+        [tails[:, border - reach :], glu_rows, heads[:, :reach]], axis=1
+    ).astype(f32)
+    taps = jnp.concatenate([conv_weight, channel_gain[None]], axis=0)
+    taps = lax.dynamic_slice_in_dim(taps, group * channels, channels, axis=1)
+    conv_sum = jnp.zeros((RING, tok_rows, channels), f32)
+    for offset in range(CONV_W):
+        conv_sum = conv_sum + taps[offset] * padded[:, offset : offset + tok_rows]
+    conv_sum = conv_sum.reshape(rows, channels)
+    squares = jnp.sum(conv_sum * conv_sum, axis=1).reshape(rows // 128, 128)
+    squares = jnp.pad(squares, ((0, -squares.shape[0] % 8), (0, 0)))
+    shared = exchange(
+        squares_kernel,
+        2,
+        shape((2 * RING,) + squares.shape, f32),
+        [DMA((1,)), DMA((7,)), DMA((7,))],
+        squares,
+    )
+    squares = jnp.sum(shared, axis=0).reshape(-1)[:rows]
+    scaled = conv_sum * lax.rsqrt(squares / C_CH + EPS)[:, None] * taps[CONV_W]
+    conv_out = jax.nn.silu(scaled).astype(bf16)
+
+    model = RING * PLANE * depth
+    mixed = contract_last(att_out, attn_all.reshape(model, q_cols)) + contract_last(
+        conv_out, conv_all.reshape(model, channels)
+    )
+    mixed = mixed.astype(bf16).reshape(RING, 2, tok_rows // 2, model)
+    block = mixed.shape[2:]
+    return exchange(
+        sum_kernel,
+        3,
+        shape(block, bf16),
+        [
+            pltpu.VMEM((4,) + block, bf16),
+            pltpu.VMEM((3,) + block, bf16),
+            pltpu.VMEM((3,) + block, bf16),
+            DMA((4,)),
+            DMA((4,)),
+            DMA((3,)),
+            DMA((3,)),
+        ],
+        mixed,
+    )
+
+
+def body_for(mesh):
+    if mesh.shape["sp"] == RING * PLANE and mesh.shape["tp"] == 2:
+        return grouped
+    return local
+
+
 def solution(mesh):
     return jax.shard_map(
-        local,
+        body_for(mesh),
         mesh=mesh,
         in_specs=(
             P("sp", "tp"),

time: 661 us -> 206 us (0.31)
  the two profiles are of different devices: /device:TPU:0 before, /device:TPU:9 now
where the time goes in v2:
time: 206 us; the launch traced here: 205 us
  Pallas kernels  166 us (81%)
  local copies, waits for them, and re-layouts  18.7 us (9%)
  other arithmetic  10.7 us (5%)
  matrix products  8.84 us (4%)
    pallas_call x4, Pallas kernels, exchange(): pl.pallas_call(kernel, out_shape=shapes, in_specs=[pl.BlockSpec(memory_sp...  166 us
    unnamed x26, local copies, waits for them, and re-layouts  6.77 us
    dot_general x2, matrix products, contract_last(): lax.dot_general(left, right, (((1,), (1,)), ((), ())), preferred_element_...  4.17 us

profile of v2, /device:TPU:9, one launch (start us, length us, event | category | flops | bytes accessed | tf_op | source)
XLA Modules:
  0.0 205.1 jit_solution(11943396665735837093)
XLA Ops:
  0.0 1.3 dynamic_slice.6.lam_ref
  1.3 0.7 mul.432
  2.0 0.7 mul.433
  2.6 0.7 broadcast_in_dim.2
  3.3 0.9 fusion.42
  4.2 0.6 fusion.48
  4.8 1.1 copy.34
  5.9 0.1 copy.36
  6.1 1.1 copy.35
  7.2 0.1 copy.37
  7.3 0.9 maximum_bitcast_fusion.1.g_ref
  8.2 1.1 copy.45
  9.3 0.8 copy.46
  10.1 57.9 %gather_kernel.1 = (bf16[4,4,128,896]{3,2,1,0:T(8,128)(2,1)}, bf16[2,4,224,1024]{3,2,1,0:T(8,128)(2,1)}) custom-call(bf16[128,1024]{1,0:T(8,128)(2,1)} %q_ref.1, bf16[128,512]{1,0:T(8,128)(2,1)} %k_ref.1, bf16[128,512]{1,0:T(8,128)(2,1)} %v_ref.1, bf16[4,128,384]{2,1,0:T(8,128)(2,1)} %maximum_bitcast_fusion.1.g_ref, bf16[224,1024]{1,0:T(8,128)(2,1)} %t_ref.1), custom_call_target="tpu_custom_call" | custom-call | tf_op jit(solution)/shard_map/gather_kernel/pallas_call | solution.py:530
  68.1 2.5 %fusion.46 = (bf16[1,4,224,1024]{3,2,1,0:T(8,128)(2,1)S(1)}, bf16[1,4,224,1024]{3,2,1,0:T(8,128)(2,1)S(1)}) fusion(bf16[2,4,224,1024]{3,2,1,0:T(8,128)(2,1)} %get-tuple-element.11), kind=kLoop, calls=%fused_computation.108 | loop fusion | bytes 7340032 | tf_op jit(solution)/shard_map/slice | solution.py:597
  70.6 0.8 fusion
  71.4 1.2 copy-done.8
  72.6 2.1 %fusion.5 = f32[896,384]{0,1:T(8,128)S(1)} fusion(bf16[2048,896]{1,0:T(8,128)(2,1)S(1)} %bitcast.133, f32[2048]{0:T(1024)S(1)} %copy-done.9, f32[896]{0:T(1024)S(1)} %add_rsqrt_fusion.3, bf16[896,1024]{1,0:T(8,128)(2,1)S(1)} %bitcast.87, bf16[896,1024]{1,0:T(8,128)(2,1)S(1)} %bitcast.84), kind=kOutput, calls=%fused_computation.9 | convolution fusion | flops 1422131200 | bytes 6631424 | tf_op jit(solution)/shard_map/dot_general | solution.py:602
  74.6 2.6 %fusion.3 = f32[896,512]{0,1:T(8,128)S(1)} fusion(bf16[2048,896]{1,0:T(8,128)(2,1)S(1)} %bitcast.134, f32[2048]{0:T(1024)S(1)} %copy-done.9, f32[896]{0:T(1024)S(1)} %add_rsqrt_fusion.3, bf16[896,1024]{1,0:T(8,128)(2,1)S(1)} %bitcast.88, bf16[896,1024]{1,0:T(8,128)(2,1)S(1)} %bitcast.85), kind=kOutput, calls=%fused_computation.7 | convolution fusion | flops 1891893248 | bytes 7614464 | tf_op jit(solution)/shard_map/dot_general | solution.py:601
  77.3 0.2 fusion.41
  77.5 0.1 multiply_reduce_fusion.1
  77.6 0.2 copy.44
  77.8 0.6 pad_maximum_fusion.2.edge_ref
  78.5 0.2 copy.49
  78.7 0.2 multiply_convert_fusion.1
  78.9 0.2 copy.48
  79.2 0.2 copy.41
  79.5 0.2 copy.42
  79.7 0.7 multiply_convert_fusion.2
  80.4 0.8 pad_maximum_fusion.1.kv_ref
  81.2 0.1 pad_bitcast_fusion
  81.4 0.1 maximum_bitcast_fusion
  81.5 1.3 copy.39
  82.8 47.8 %attend_kernel.1 = (bf16[896,256]{1,0:T(8,128)(2,1)}, bf16[2,4,16,192]{3,2,1,0:T(8,128)(2,1)}, bf16[4,4,128,256]{3,2,1,0:T(8,128)(2,1)}, bf16[4,4,128,192]{3,2,1,0:T(8,128)(2,1)}) custom-call(f32[2]{0:T(128)} %dynamic_slice.6.lam_ref, f32[1,128]{1,0:T(1,128)} %bitcast.132, bf16[4,896,128]{2,1,0:T(8,128)(2,1)} %bitcast.89, ...), custom_call_target="tpu_custom_call" | custom-call | tf_op jit(solution)/shard_map/attend_kernel/pallas_call | solution.py:530
  130.6 0.8 slice_bitcast_fusion.7
  131.3 0.8 slice_bitcast_fusion.5
  132.2 0.1 maximum_convert_fusion
  132.3 4.0 %multiply_reduce_fusion = (f32[4,224]{1,0:T(4,128)S(1)}, f32[4,224,192]{2,1,0:T(8,128)S(1)}) fusion(f32[4,254,192]{2,1,0:T(8,128)S(1)} %maximum_convert_fusion, f32[192]{0:T(256)S(1)} %bitcast.101, f32[192]{0:T(256)S(1)} %bitcast.102, f32[192]{0:T(256)S(1)} %bitcast.103, f32[192]{0:T(256)S(1)} %bitcast.104, f32[192]{0:T(256)S(1)} %bitcast.105, ...), kind=kLoop, calls=%fused_computation.74 | loop fusion | flops 10837120 | bytes 22047488 | tf_op jit(solution)/shard_map/reduce_sum | solution.py:662
  136.4 0.1 reshape.136
  136.5 0.6 pad.16.sq_ref
  137.1 12.8 %squares_kernel.1 = f32[8,8,128]{2,1,0:T(8,128)} custom-call(f32[8,128]{1,0:T(8,128)} %pad.16.sq_ref), custom_call_target="tpu_custom_call" | custom-call | tf_op jit(solution)/shard_map/squares_kernel/pallas_call | solution.py:530
  149.9 0.8 reduce_sum.49
  150.6 0.1 rsqrt.38
  150.7 0.3 multiply_convert_fusion
  151.1 1.1 fusion.49
  152.3 3.0 %add_convert_fusion = bf16[896,2048]{1,0:T(8,128)(2,1)} fusion(f32[896,2048]{1,0:T(8,128)S(1)} %fusion.49, bf16[896,192]{1,0:T(8,128)(2,1)S(1)} %bitcast.93, bf16[2048,192]{1,0:T(8,128)(2,1)S(1)} %bitcast.94), kind=kOutput, calls=%fused_computation.5 | convolution fusion | flops 708313088 | bytes 12140544 | tf_op jit(solution)/shard_map/dot_general | solution.py:39
  155.3 47.9 %sum_kernel.1 = bf16[112,2048]{1,0:T(8,128)(2,1)} custom-call(bf16[4,2,112,2048]{3,2,1,0:T(8,128)(2,1)} %bitcast.82), custom_call_target="tpu_custom_call" | custom-call | tf_op jit(solution)/shard_map/sum_kernel/pallas_call | solution.py:530
  203.3 1.8 copy.51
  (33 shorter events, 0.4 us)
Async XLA Ops:
  70.5 2.0 copy-start.8
  70.5 2.0 copy-start.9
  77.3 1.4 copy-start.7
  81.3 51.0 %copy-start.3 = (f32[1,192]{1,0:T(1,128)S(1)}, f32[1,192]{1,0:T(1,128)}, u32[]{:S(2)}) copy-start(f32[1,192]{1,0:T(1,128)} %get-tuple-element.57) | copy-start | bytes 2308
  81.3 51.0 %copy-start.4 = (f32[1,192]{1,0:T(1,128)S(1)}, f32[1,192]{1,0:T(1,128)}, u32[]{:S(2)}) copy-start(f32[1,192]{1,0:T(1,128)} %get-tuple-element.58) | copy-start | bytes 2308
  81.3 51.0 %copy-start.5 = (f32[1,192]{1,0:T(1,128)S(1)}, f32[1,192]{1,0:T(1,128)}, u32[]{:S(2)}) copy-start(f32[1,192]{1,0:T(1,128)} %get-tuple-element.59) | copy-start | bytes 2308
  81.3 51.0 %copy-start.6 = (f32[1,192]{1,0:T(1,128)S(1)}, f32[1,192]{1,0:T(1,128)}, u32[]{:S(2)}) copy-start(f32[1,192]{1,0:T(1,128)} %get-tuple-element.60) | copy-start | bytes 2308
  132.3 18.7 %copy-start.1 = (bf16[4,4,128,256]{3,2,1,0:T(8,128)(2,1)S(1)}, bf16[4,4,128,256]{3,2,1,0:T(8,128)(2,1)}, u32[]{:S(2)}) copy-start(bf16[4,4,128,256]{3,2,1,0:T(8,128)(2,1)} %get-tuple-element.14) | copy-start | bytes 3145732
  132.3 18.7 %copy-start.2 = (bf16[896,256]{1,0:T(8,128)(2,1)S(1)}, bf16[896,256]{1,0:T(8,128)(2,1)}, u32[]{:S(2)}) copy-start(bf16[896,256]{1,0:T(8,128)(2,1)} %get-tuple-element.13) | copy-start | bytes 1376260
  151.1 1.2 copy-start

commit v3 on v2

--- a/solution.py
+++ b/solution.py
@@ -230,9 +230,11 @@
     local_copies.append(pltpu.make_async_copy(t_ref, tout.at[core, group], own.at[4]))
     for copy in local_copies:
         copy.start()
+    pieces = [list(segments(chip // PLANE)) for chip in line]
     first = []
-    for hop, chip in enumerate(line):
-        for i, (piece, place) in enumerate(segments(chip // PLANE)):
+    for i in range(4):
+        for hop, chip in enumerate(line):
+            piece, place = pieces[hop][i]
             first.append(
                 send(piece, place, ws.at[hop * 4 + i], wr.at[hop * 4 + i], at(chip, core))
             )
@@ -280,14 +282,27 @@
 
     for copy in local_copies:
         copy.wait()
-    for copy in first:
-        copy.wait_recv()
-    mine = wout.at[:, spot]
-    ring = [
-        send(mine, mine, xs.at[0], xr.at[0], at(x_peer, core)),
-        send(mine, mine, xs.at[1], xr.at[1], at(y_peer, core)),
-    ]
+    edge = wout.shape[3] - g_ref.shape[2]
+    parts = (pl.ds(0, edge), pl.ds(edge, g_ref.shape[2]))
+    ring = []
+    for part_no, arrivals in enumerate((first[:9], first[9:])):
+        for copy in arrivals:
+            copy.wait_recv()
+        mine = wout.at[:, spot, :, parts[part_no]]
+        sem = part_no * 4
+        ring.append(send(mine, mine, xs.at[sem], xr.at[sem], at(x_peer, core)))
+        ring.append(send(mine, mine, xs.at[sem + 1], xr.at[sem + 1], at(y_peer, core)))
+    cut = RING // 2
+    relays = []
     for step in range(RING - 1):
+        if step < len(parts):
+            sem = step * 4
+            ring[2 * step].wait_recv()
+            piece = wout.at[pl.ds(0, cut), x_peer % PLANE, :, parts[step]]
+            relays.append(send(piece, piece, xs.at[sem + 2], xr.at[sem + 2], at(y_peer, core)))
+            ring[2 * step + 1].wait_recv()
+            piece = wout.at[pl.ds(cut, cut), y_peer % PLANE, :, parts[step]]
+            relays.append(send(piece, piece, xs.at[sem + 3], xr.at[sem + 3], at(x_peer, core)))
         for upward in (True, False):
 
             @pl.when(receives(step, upward))
@@ -301,13 +316,6 @@
                 def _():
                     token_copy(step + 1, upward).start()
 
-    cut = RING // 2
-    ring[0].wait_recv()
-    piece = wout.at[pl.ds(0, cut), x_peer % PLANE]
-    ring.append(send(piece, piece, xs.at[2], xr.at[2], at(y_peer, core)))
-    ring[1].wait_recv()
-    piece = wout.at[pl.ds(cut, cut), y_peer % PLANE]
-    ring.append(send(piece, piece, xs.at[3], xr.at[3], at(x_peer, core)))
     for hop in range(RING):
         partner_copy(hop).wait()
     for step in range(RING - 1):
@@ -317,9 +325,9 @@
             def _():
                 token_copy(step, upward).wait_send()
 
-    ring[2].wait_recv()
-    ring[3].wait_recv()
-    for copy in first + ring:
+    for copy in relays:
+        copy.wait_recv()
+    for copy in first + ring + relays:
         copy.wait_send()
 
 
@@ -343,37 +351,99 @@
         copy.wait()
 
 
-def sum_kernel(p_ref, o_ref, near, mid, far, ns, nr, fs, fr):
+def sum_kernel(p_ref, o_ref, near, mid, below, above, ns, nr, us, ur, ds, dr):
     core, group, spot, x_peer, y_peer, diagonal, line = where_am_i()
     me = group * PLANE + spot
     other = 1 - core
-    chips = [line[1], line[0], line[2], me]
-    greet([at(me, other)] + [at(chip, core) for chip in chips[:3]])
-    inner = [
-        send(
-            p_ref.at[chip // PLANE, other],
-            near.at[slot],
-            ns.at[slot],
-            nr.at[slot],
-            at(me, other),
-        )
-        for slot, chip in enumerate(chips)
-    ]
-    outer = []
-    for slot, chip in enumerate(chips):
-        inner[slot].wait_recv()
-        total = p_ref[chip // PLANE, core].astype(jnp.float32) + near[slot].astype(jnp.float32)
-        if slot < 3:
-            mid[slot] = total.astype(jnp.bfloat16)
-            outer.append(
-                send(mid.at[slot], far.at[slot], fs.at[slot], fr.at[slot], at(chip, core))
-            )
-    for slot in range(3):
-        outer[slot].wait_recv()
-        total = total + far[slot].astype(jnp.float32)
-    o_ref[...] = total.astype(o_ref.dtype)
-    for copy in inner + outer:
-        copy.wait_send()
+    greet([at(me, other)] + [at(chip, core) for chip in line])
+    upper = (2 * group) // RING
+
+    def inner(goal):
+        return pltpu.make_async_remote_copy(
+            src_ref=p_ref.at[goal, other],
+            dst_ref=near.at[goal],
+            send_sem=ns.at[goal],
+            recv_sem=nr.at[goal],
+            device_id=at(me, other),
+            device_id_type=pl.DeviceIdType.MESH,
+        )
+
+    for turn in range(RING):
+        inner(upper * turn + (1 - upper) * (RING - 1 - turn)).start()
+
+    def hop(goal, upward):
+        move = 1 if upward else RING - 1
+        return pltpu.make_async_remote_copy(
+            src_ref=mid.at[goal],
+            dst_ref=(below if upward else above).at[goal],
+            send_sem=(us if upward else ds).at[goal],
+            recv_sem=(ur if upward else dr).at[goal],
+            device_id=at(((group + move) % RING) * PLANE + spot, core),
+            device_id_type=pl.DeviceIdType.MESH,
+        )
+
+    def own(goal):
+        return p_ref[goal, core].astype(jnp.float32) + near[goal].astype(jnp.float32)
+
+    def move_on(goal, upward):
+        start = 0 if upward else RING - 1
+        passes = group < goal if upward else group > goal
+        came = below if upward else above
+
+        @pl.when(jnp.logical_and(passes, group == start))
+        def _():
+            mid[goal] = own(goal).astype(jnp.bfloat16)
+            hop(goal, upward).start()
+
+        @pl.when(jnp.logical_and(passes, group != start))
+        def _():
+            hop(goal, upward).wait_recv()
+            mid[goal] = (own(goal) + came[goal].astype(jnp.float32)).astype(jnp.bfloat16)
+            hop(goal, upward).start()
+
+    @pl.when(upper == 0)
+    def _():
+        for goal in range(RING - 1, -1, -1):
+            inner(goal).wait_recv()
+            if goal > 0:
+                move_on(goal, True)
+        for goal in range(RING // 2 - 1):
+            move_on(goal, False)
+
+    @pl.when(upper == 1)
+    def _():
+        for goal in range(RING):
+            inner(goal).wait_recv()
+            if goal < RING - 1:
+                move_on(goal, False)
+        for goal in range(RING - 1, RING // 2, -1):
+            move_on(goal, True)
+
+    for goal in range(RING):
+
+        @pl.when(group == goal)
+        def _():
+            if goal > 0:
+                hop(goal, True).wait_recv()
+            if goal < RING - 1:
+                hop(goal, False).wait_recv()
+            total = own(goal)
+            if goal > 0:
+                total = total + below[goal].astype(jnp.float32)
+            if goal < RING - 1:
+                total = total + above[goal].astype(jnp.float32)
+            o_ref[...] = total.astype(o_ref.dtype)
+
+    for goal in range(RING):
+        inner(goal).wait_send()
+
+        @pl.when(group < goal)
+        def _():
+            hop(goal, True).wait_send()
+
+        @pl.when(group > goal)
+        def _():
+            hop(goal, False).wait_send()
 
 
 def attend_kernel(
@@ -489,6 +559,9 @@
         ring.append(send(block, block, xs.at[2 + i], xr.at[2 + i], at(y_peer, core)))
     attend(kv_all.at[0], False)
     attend(kv_all.at[1], False)
+    keys[2].wait_recv()
+    keys[3].wait_recv()
+    attend(kv_all.at[2], False)
     cut = RING // 2
     for i, buf in enumerate((a_out, c_out)):
         ring[2 * i].wait_recv()
@@ -497,9 +570,6 @@
         ring[2 * i + 1].wait_recv()
         piece = buf.at[pl.ds(cut, cut), y_peer % PLANE]
         ring.append(send(piece, piece, xs.at[6 + i], xr.at[6 + i], at(x_peer, core)))
-    keys[2].wait_recv()
-    keys[3].wait_recv()
-    attend(kv_all.at[2], False)
     for head in range(q_ref.shape[0] // 2):
 
         @pl.loop(0, 2)
@@ -510,7 +580,7 @@
                 / jnp.sum(sums[2 * head + pair, span], axis=1, keepdims=True)
                 for pair in range(2)
             ]
-            att = ratios[0] - lam_ref[head] * ratios[1]
+            att = ratios[0] - lam_ref[group * (q_ref.shape[0] // 2) + head] * ratios[1]
             att = rms_scale(att, gain_ref[...]) * (1.0 - LAMBDA_INIT)
             o_ref[span, head * width : (head + 1) * width] = att.astype(o_ref.dtype)
 
@@ -526,12 +596,15 @@
 DMA = pltpu.SemaphoreType.DMA
 
 
-def exchange(kernel, number, shapes, scratch, *operands, scalars=0):
+def exchange(kernel, number, shapes, scratch, *operands, scalars=0, far=()):
     return pl.pallas_call(
         kernel,
         out_shape=shapes,
         in_specs=[pl.BlockSpec(memory_space=pltpu.SMEM)] * scalars
-        + [VMEM] * (len(operands) - scalars),
+        + [
+            pl.BlockSpec(memory_space=pl.ANY) if i in far else VMEM
+            for i in range(scalars, len(operands))
+        ],
         out_specs=jax.tree.map(lambda _: VMEM, shapes),
         scratch_shapes=scratch,
         compiler_params=pltpu.CompilerParams(
@@ -582,7 +655,7 @@
             shape((RING, PLANE, depth, columns), bf16),
             shape((2, RING, tok_rows, half_width), bf16),
         ),
-        [DMA((5,)), DMA((12,)), DMA((12,)), DMA((4,)), DMA((4,))]
+        [DMA((5,)), DMA((12,)), DMA((12,)), DMA((8,)), DMA((8,))]
         + [DMA((3,))] * 4
         + [DMA((4,))] * 2,
         query_weight,
@@ -590,6 +663,7 @@
         value_weight,
         quarters(glu_value_weight, glu_gate_weight),
         tokens,
+        far=(0, 1, 2, 4),
     )
     w_all = w_all.reshape(RING * PLANE * depth, columns)
     rows = RING * tok_rows
@@ -614,7 +688,6 @@
     reach = CONV_W // 2
     border = 16
     edges = jnp.stack([glu_rows[:, :border], glu_rows[:, tok_rows - border :]])
-    lam = lax.dynamic_slice_in_dim(lambdas, group * q_heads, q_heads, axis=0)
     att_out, halo, attn_all, conv_all = exchange(
         attend_kernel,
         1,
@@ -638,7 +711,7 @@
             DMA((8,)),
             DMA((8,)),
         ],
-        lam,
+        lambdas,
         head_gain.reshape(1, width),
         queries,
         kv,
@@ -646,6 +719,7 @@
         attn_out_weight,
         quarters(conv_out_weight),
         scalars=1,
+        far=(5,),
     )
     blank = jnp.zeros_like(halo[0, :1])
     tails = jnp.where(spot > 0, halo[0], jnp.concatenate([blank, halo[0, :-1]]))
@@ -682,15 +756,7 @@
         sum_kernel,
         3,
         shape(block, bf16),
-        [
-            pltpu.VMEM((4,) + block, bf16),
-            pltpu.VMEM((3,) + block, bf16),
-            pltpu.VMEM((3,) + block, bf16),
-            DMA((4,)),
-            DMA((4,)),
-            DMA((3,)),
-            DMA((3,)),
-        ],
+        [pltpu.VMEM((RING,) + block, bf16)] * 4 + [DMA((RING,))] * 6,
         mixed,
     )
 

time: 206 us -> 191 us (0.927)
  the two profiles are of different devices: /device:TPU:9 before, /device:TPU:0 now
where the time goes in v3:
time: 191 us; the launch traced here: 190 us
  Pallas kernels  153 us (80%)
  local copies, waits for them, and re-layouts  17.4 us (9%)
  other arithmetic  10.7 us (6%)
  matrix products  8.84 us (5%)
    pallas_call x4, Pallas kernels, exchange(): pl.pallas_call(kernel, out_shape=shapes, in_specs=[pl.BlockSpec(memory_sp...  153 us
    unnamed x26, local copies, waits for them, and re-layouts  6.77 us
    dot_general x2, matrix products, contract_last(): lax.dot_general(left, right, (((1,), (1,)), ((), ())), preferred_element_...  4.17 us
    reduce_sum x1, other arithmetic, grouped(): squares = jnp.sum(conv_sum * conv_sum, axis=1).reshape(rows // 128, 128)  4.05 us

profile of v3, /device:TPU:0, one launch (start us, length us, event | category | flops | bytes accessed | tf_op | source)
XLA Modules:
  0.0 189.9 jit_solution(11670389703694544301)
XLA Ops:
  0.0 0.7 mul.428
  0.7 0.7 mul.429
  1.3 0.7 broadcast_in_dim.2
  2.0 0.9 fusion.42
  2.9 0.6 fusion.48
  3.5 1.1 copy.34
  4.6 0.1 copy.36
  4.8 1.1 copy.35
  5.8 0.1 copy.37
  6.0 0.9 maximum_bitcast_fusion.1.g_ref
  6.9 1.1 copy.45
  8.0 0.8 copy.46
  8.8 61.9 %gather_kernel.1 = (bf16[4,4,128,896]{3,2,1,0:T(8,128)(2,1)}, bf16[2,4,224,1024]{3,2,1,0:T(8,128)(2,1)}) custom-call(bf16[128,1024]{1,0:T(8,128)(2,1)} %q_ref.1, bf16[128,512]{1,0:T(8,128)(2,1)} %k_ref.1, bf16[128,512]{1,0:T(8,128)(2,1)} %v_ref.1, bf16[4,128,384]{2,1,0:T(8,128)(2,1)} %maximum_bitcast_fusion.1.g_ref, bf16[224,1024]{1,0:T(8,128)(2,1)} %t_ref.1), custom_call_target="tpu_custom_call" | custom-call | tf_op jit(solution)/shard_map/gather_kernel/pallas_call | solution.py:600
  70.7 2.5 %fusion.46 = (bf16[1,4,224,1024]{3,2,1,0:T(8,128)(2,1)S(1)}, bf16[1,4,224,1024]{3,2,1,0:T(8,128)(2,1)S(1)}) fusion(bf16[2,4,224,1024]{3,2,1,0:T(8,128)(2,1)} %get-tuple-element.11), kind=kLoop, calls=%fused_computation.108 | loop fusion | bytes 7340032 | tf_op jit(solution)/shard_map/slice | solution.py:671
  73.2 0.8 fusion
  74.0 1.2 copy-done.8
  75.2 2.1 %fusion.5 = f32[896,384]{0,1:T(8,128)S(1)} fusion(bf16[2048,896]{1,0:T(8,128)(2,1)S(1)} %bitcast.133, f32[2048]{0:T(1024)S(1)} %copy-done.9, f32[896]{0:T(1024)S(1)} %add_rsqrt_fusion.3, bf16[896,1024]{1,0:T(8,128)(2,1)S(1)} %bitcast.87, bf16[896,1024]{1,0:T(8,128)(2,1)S(1)} %bitcast.84), kind=kOutput, calls=%fused_computation.9 | convolution fusion | flops 1422131200 | bytes 6631424 | tf_op jit(solution)/shard_map/dot_general | solution.py:676
  77.3 2.6 %fusion.3 = f32[896,512]{0,1:T(8,128)S(1)} fusion(bf16[2048,896]{1,0:T(8,128)(2,1)S(1)} %bitcast.134, f32[2048]{0:T(1024)S(1)} %copy-done.9, f32[896]{0:T(1024)S(1)} %add_rsqrt_fusion.3, bf16[896,1024]{1,0:T(8,128)(2,1)S(1)} %bitcast.88, bf16[896,1024]{1,0:T(8,128)(2,1)S(1)} %bitcast.85), kind=kOutput, calls=%fused_computation.7 | convolution fusion | flops 1891893248 | bytes 7614464 | tf_op jit(solution)/shard_map/dot_general | solution.py:675
  79.9 0.2 fusion.41
  80.1 0.1 multiply_reduce_fusion.1
  80.3 0.2 copy.44
  80.5 0.6 pad_maximum_fusion.2.edge_ref
  81.2 0.2 copy.49
  81.3 0.2 multiply_convert_fusion.1
  81.6 0.2 copy.48
  81.9 0.2 copy.41
  82.2 0.2 copy.42
  82.4 0.7 multiply_convert_fusion.2
  83.1 0.8 pad_maximum_fusion.1.kv_ref
  83.9 0.1 pad_bitcast_fusion
  84.0 0.1 maximum_bitcast_fusion
  84.1 1.3 copy.39
  85.4 41.8 %attend_kernel.1 = (bf16[896,256]{1,0:T(8,128)(2,1)}, bf16[2,4,16,192]{3,2,1,0:T(8,128)(2,1)}, bf16[4,4,128,256]{3,2,1,0:T(8,128)(2,1)}, bf16[4,4,128,192]{3,2,1,0:T(8,128)(2,1)}) custom-call(f32[8]{0:T(128)} %lam_ref.1, f32[1,128]{1,0:T(1,128)} %bitcast.132, bf16[4,896,128]{2,1,0:T(8,128)(2,1)} %bitcast.89, bf16[896,256]{1,0:T(8,128)(2,1)} %pad_maximum_fusion.1.kv_ref, ...), custom_call_target="tpu_custom_call" | custom-call | tf_op jit(solution)/shard_map/attend_kernel/pallas_call | solution.py:600
  127.2 0.8 slice_bitcast_fusion.7
  128.0 0.8 slice_bitcast_fusion.5
  128.8 0.1 maximum_convert_fusion
  129.0 4.0 %multiply_reduce_fusion = (f32[4,224]{1,0:T(4,128)S(1)}, f32[4,224,192]{2,1,0:T(8,128)S(1)}) fusion(f32[4,254,192]{2,1,0:T(8,128)S(1)} %maximum_convert_fusion, f32[192]{0:T(256)S(1)} %bitcast.101, f32[192]{0:T(256)S(1)} %bitcast.102, f32[192]{0:T(256)S(1)} %bitcast.103, f32[192]{0:T(256)S(1)} %bitcast.104, f32[192]{0:T(256)S(1)} %bitcast.105, ...), kind=kLoop, calls=%fused_computation.74 | loop fusion | flops 10837120 | bytes 22047488 | tf_op jit(solution)/shard_map/reduce_sum | solution.py:736
  133.0 0.1 reshape.136
  133.1 0.6 pad.16.sq_ref
  133.7 6.9 %squares_kernel.1 = f32[8,8,128]{2,1,0:T(8,128)} custom-call(f32[8,128]{1,0:T(8,128)} %pad.16.sq_ref), custom_call_target="tpu_custom_call" | custom-call | tf_op jit(solution)/shard_map/squares_kernel/pallas_call | solution.py:600
  140.6 0.8 reduce_sum.49
  141.4 0.1 rsqrt.38
  141.4 0.3 multiply_convert_fusion
  141.8 1.2 fusion.49
  143.0 0.1 copy-done
  143.0 3.0 %add_convert_fusion = bf16[896,2048]{1,0:T(8,128)(2,1)} fusion(f32[896,2048]{1,0:T(8,128)S(1)} %fusion.49, bf16[896,192]{1,0:T(8,128)(2,1)S(1)} %bitcast.93, bf16[2048,192]{1,0:T(8,128)(2,1)S(1)} %bitcast.94), kind=kOutput, calls=%fused_computation.5 | convolution fusion | flops 708313088 | bytes 12140544 | tf_op jit(solution)/shard_map/dot_general | solution.py:39
  146.0 42.1 %sum_kernel.1 = bf16[112,2048]{1,0:T(8,128)(2,1)} custom-call(bf16[4,2,112,2048]{3,2,1,0:T(8,128)(2,1)} %bitcast.82), custom_call_target="tpu_custom_call" | custom-call | tf_op jit(solution)/shard_map/sum_kernel/pallas_call | solution.py:600
  188.1 1.8 copy.51
  (32 shorter events, 0.4 us)
Async XLA Ops:
  73.2 2.0 %copy-start.8 = (bf16[4,4,128,896]{3,2,1,0:T(8,128)(2,1)S(1)}, bf16[4,4,128,896]{3,2,1,0:T(8,128)(2,1)}, u32[]{:S(2)}) copy-start(bf16[4,4,128,896]{3,2,1,0:T(8,128)(2,1)} %get-tuple-element.12) | copy-start | bytes 11010052
  73.2 2.0 %copy-start.9 = (f32[2048]{0:T(1024)S(1)}, f32[2048]{0:T(1024)}, u32[]{:S(2)}) copy-start(f32[2048]{0:T(1024)} %param.16) | copy-start | bytes 24580
  79.9 1.4 copy-start.7
  84.0 44.9 %copy-start.3 = (f32[1,192]{1,0:T(1,128)S(1)}, f32[1,192]{1,0:T(1,128)}, u32[]{:S(2)}) copy-start(f32[1,192]{1,0:T(1,128)} %get-tuple-element.57) | copy-start | bytes 2308
  84.0 44.9 %copy-start.4 = (f32[1,192]{1,0:T(1,128)S(1)}, f32[1,192]{1,0:T(1,128)}, u32[]{:S(2)}) copy-start(f32[1,192]{1,0:T(1,128)} %get-tuple-element.58) | copy-start | bytes 2308
  84.0 44.9 %copy-start.5 = (f32[1,192]{1,0:T(1,128)S(1)}, f32[1,192]{1,0:T(1,128)}, u32[]{:S(2)}) copy-start(f32[1,192]{1,0:T(1,128)} %get-tuple-element.59) | copy-start | bytes 2308
  84.0 44.9 %copy-start.6 = (f32[1,192]{1,0:T(1,128)S(1)}, f32[1,192]{1,0:T(1,128)}, u32[]{:S(2)}) copy-start(f32[1,192]{1,0:T(1,128)} %get-tuple-element.60) | copy-start | bytes 2308
  129.0 12.8 %copy-start.1 = (bf16[4,4,128,256]{3,2,1,0:T(8,128)(2,1)S(1)}, bf16[4,4,128,256]{3,2,1,0:T(8,128)(2,1)}, u32[]{:S(2)}) copy-start(bf16[4,4,128,256]{3,2,1,0:T(8,128)(2,1)} %get-tuple-element.14) | copy-start | bytes 3145732
  129.0 12.8 %copy-start.2 = (bf16[896,256]{1,0:T(8,128)(2,1)S(1)}, bf16[896,256]{1,0:T(8,128)(2,1)}, u32[]{:S(2)}) copy-start(bf16[896,256]{1,0:T(8,128)(2,1)} %get-tuple-element.13) | copy-start | bytes 1376260
  141.8 1.2 copy-start
